TPU v7x, 512 devices: a 8x2x16 block of a 8x16x16 slice. The times are simulated.
512 devices in a mesh: grp: 2 (over y), fs: 16 (over z), tp: 16 (over x, core).
Axes of the slice: x: 8, y: 2, z: 16, core: 2. Of those that a mesh axis runs over, the one named last changes fastest.
The devices are a block of a 8x16x16 slice.
Arguments:
- tokens: bfloat16 [4096, 2048], P(('grp', 'fs'), 'tp'), parts along dimension 0, may hold values from -40 to 40
- norm_gain: float32 [2048], P('tp'), may hold values from 0.1 to 1.9
- expert_ids: int32 [4096, 8], P(('grp', 'fs')), parts along dimension 0, may hold values from 0 to 63, all different within a row; in each aligned block of 128 rows (0 to 127, 128 to 255, ...) at most 24 rows name the same one
- route_scores: float32 [4096, 8], P(('grp', 'fs')), parts along dimension 0, may hold values from 0.1 to 1
- gate_weight: float32 [64, 512, 2048], P(None, 'fs', 'tp'), may hold values from -0.125 to 0.125
- up_weight: float32 [64, 512, 2048], P(None, 'fs', 'tp'), may hold values from -0.125 to 0.125
- down_weight: float32 [64, 512, 2048], P(None, 'fs', 'tp'), may hold values from -0.25 to 0.25
- shared_gate: float32 [512, 2048], P('fs', 'tp'), may hold values from -0.125 to 0.125
- shared_up: float32 [512, 2048], P('fs', 'tp'), may hold values from -0.125 to 0.125
- shared_down: float32 [512, 2048], P('fs', 'tp'), may hold values from -0.25 to 0.25
Outputs:
- gate_served: bfloat16 [128, 512, 2048], P(('grp', 'fs'), None, 'tp'), parts along dimension 0
- up_served: bfloat16 [128, 512, 2048], P(('grp', 'fs'), None, 'tp'), parts along dimension 0
- down_served: bfloat16 [128, 512, 2048], P(('grp', 'fs'), None, 'tp'), parts along dimension 0
- shared_gate_served: bfloat16 [1024, 2048], P('grp', 'tp'), parts along dimension 0
- shared_up_served: bfloat16 [1024, 2048], P('grp', 'tp'), parts along dimension 0
- shared_down_served: bfloat16 [1024, 2048], P('grp', 'tp'), parts along dimension 0
- layer_output: bfloat16 [4096, 2048], P(('grp', 'fs'), 'tp'), parts along dimension 0
There are 2 independent parts, one for each index of `grp`. A program takes and returns all parts, laid end to end along the dimension named above; an argument that names none is the same for every part. Nothing has to cross between parts.
Inputs may be any that keep to these rules, and one draw needn't show every extreme that they name: `expert_ids`: each row names 8 different experts. Among the rows of one index of fs no expert is named more than 24 times; in every draw some expert reaches 24 on some index of fs.
All inputs are finite; a program needn't handle non-finite values.
Results may differ from a plain program's by a relative error of at most 0.03.
Values may be sent and summed in bfloat16 or wider, within the bound.
No kernel may reach another device: no remote copies, remote signals or barrier semaphores. Data moves between devices by JAX's collectives and lax.ppermute only.
A program may use at most 64 MiB of HBM per device.

v0:
```python
import jax
import jax.numpy as jnp
from jax import lax
from jax.sharding import Mesh
from jax.sharding import PartitionSpec as P


CAPACITY = 24
TP = ("tp_0", "tp_1")


norm_eps = 1e-05
routed_scale = 2.5


def exchange(array, axis):
    return lax.all_to_all(array, axis, 0, 0, tiled=True)


def rotated(array, axis, by):
    size = lax.axis_size(axis)
    return lax.ppermute(array, axis, [(i, (i + by) % size) for i in range(size)])


def distances(axis):
    size = lax.axis_size(axis)
    return sorted(range(1, size), key=lambda by: -min(by, size - by))


def summed_parts(blocks, axis):
    at = lax.axis_index(axis)
    size = lax.axis_size(axis)
    pick = lambda i: lax.dynamic_index_in_dim(blocks, i % size, 0, keepdims=False)
    parts = [rotated(pick(at + by), axis, by) for by in distances(axis)]
    total = pick(at).astype(jnp.float32)
    for part in parts:
        total = total + part.astype(jnp.float32)
    return total


def swap_cores(array):
    return lax.ppermute(array, "tp_1", [(0, 1), (1, 0)])


def of_core(array, core, dim):
    half = array.shape[dim] // 2
    return lax.dynamic_slice_in_dim(array, core * half, half, axis=dim)


def copy_for_each(array, axis):
    size = lax.axis_size(axis)
    return exchange(jnp.broadcast_to(array[None], (size, *array.shape)), axis)


def tie(array, after):
    return lax.optimization_barrier((array, after))[0]


def with_shared(routed, shared):
    rows = jnp.broadcast_to(shared[None, None], (routed.shape[0], 1, *shared.shape))
    return jnp.concatenate([routed, rows], axis=1)


def layer(
    tokens,
    norm_gain,
    expert_ids,
    route_scores,
    gate_weight,
    up_weight,
    down_weight,
    shared_gate,
    shared_up,
    shared_down,
):
    shards = lax.axis_size("fs")
    chips = lax.axis_size("tp_0")
    core = lax.axis_index("tp_1")
    experts_all, unit_rows, slice_width = gate_weight.shape
    experts_here = experts_all // shards
    experts_core = experts_all // 2
    tok_rows, top_count = expert_ids.shape
    bf16 = jnp.bfloat16
    float32 = jnp.float32

    tok_float = tokens.astype(float32)
    sums = jnp.stack([jnp.sum(tok_float, axis=1), jnp.sum(tok_float * tok_float, axis=1)])
    row_sum, row_squares = jnp.sum(copy_for_each(sums, TP), axis=0)
    full_width = slice_width * lax.axis_size(TP)
    row_mean = row_sum / full_width
    row_var = row_squares / full_width - row_mean * row_mean
    normed = ((tok_float - row_mean[:, None]) * lax.rsqrt(row_var + norm_eps)[:, None]).astype(bf16)

    route_weight = route_scores / jnp.sum(route_scores, axis=1, keepdims=True) * routed_scale
    sent = jnp.concatenate([normed, expert_ids.T.astype(bf16), route_weight.T.astype(bf16)])
    blocks = copy_for_each(sent, "fs")

    gain = norm_gain[None, None, :]
    both_new = jnp.concatenate(
        [(gate_weight * gain).astype(bf16), (up_weight * gain).astype(bf16)], axis=1
    )
    both_shared = jnp.concatenate([shared_gate * gain[0], shared_up * gain[0]]).astype(bf16)
    down_new = down_weight.astype(bf16)
    down_shared = shared_down.astype(bf16)
    three_new = jnp.concatenate([both_new, down_new], axis=1)
    three_sent = three_new.reshape(shards, experts_here, 3 * unit_rows, slice_width)
    three_sent = with_shared(three_sent, jnp.concatenate([both_shared, down_shared]))
    served = exchange(tie(three_sent, blocks), "fs")

    def over_both(local, shared_local):
        rows = local.shape[1]
        mine = of_core(local, core, 0)
        theirs = jnp.concatenate([of_core(local, 1 - core, 0), shared_local[None]])
        theirs = swap_cores(theirs.reshape(-1, slice_width))
        theirs = theirs.reshape(-1, rows, slice_width)
        theirs_routed = theirs[:-1]
        routed = jnp.concatenate([mine, theirs_routed], axis=2)
        return routed, jnp.concatenate([shared_local, theirs[-1]], axis=1)

    both_pair, both_shared_pair = over_both(both_new, both_shared)
    down_pair, down_shared_pair = over_both(down_new, down_shared)

    blocks = tie(blocks, (both_pair, both_shared_pair, down_pair, down_shared_pair))
    own_tokens = blocks[:, :tok_rows]
    partner_tokens = swap_cores(own_tokens)
    all_tokens = jnp.concatenate([own_tokens, partner_tokens], axis=2)
    ids = blocks[:, tok_rows : tok_rows + top_count].astype(jnp.int32)
    weights = blocks[:, tok_rows + top_count :].astype(float32)

    core_experts = core * experts_core + jnp.arange(experts_core, dtype=jnp.int32)
    named = ids[:, :, None, :] == core_experts[None, None, :, None]
    chosen = jnp.any(named, axis=1)
    weight_of = jnp.sum(jnp.where(named, weights[:, :, None, :], 0.0), axis=1)
    places = jnp.arange(tok_rows, dtype=jnp.int32)
    before = places[:, None] < places[None, :]
    rank = jnp.einsum(
        "bet,tu->beu", chosen.astype(bf16), before.astype(bf16), preferred_element_type=float32
    )
    slot = jnp.where(chosen, rank.astype(jnp.int32), -1)
    in_slot = slot[:, :, None, :] == jnp.arange(CAPACITY, dtype=jnp.int32)[None, None, :, None]
    slots = experts_core * CAPACITY
    select = in_slot.astype(bf16).reshape(shards, slots, tok_rows)
    combine = jnp.where(in_slot, weight_of[:, :, None, :], 0.0).astype(bf16)
    combine = combine.reshape(shards, slots, tok_rows)

    rows_in = jnp.einsum(
        "brt,btd->brd", select, all_tokens, preferred_element_type=float32
    ).astype(bf16)
    rows_in = rows_in.reshape(shards, experts_core, CAPACITY, 2 * slice_width).transpose(1, 0, 2, 3)
    rows_in = rows_in.reshape(experts_core, shards * CAPACITY, 2 * slice_width)
    lanes = tok_rows
    groups = shards * CAPACITY // lanes

    def for_groups(weight):
        return jnp.broadcast_to(weight[:, None], (experts_core, groups, *weight.shape[1:]))

    terms = jnp.einsum(
        "egfd,egrd->egfr",
        for_groups(both_pair),
        rows_in.reshape(experts_core, groups, lanes, 2 * slice_width),
        preferred_element_type=float32,
    )
    terms = terms.astype(bf16).reshape(chips, -1, lanes)
    shared_terms = jnp.einsum(
        "fd,btd->bft",
        both_shared_pair,
        of_core(all_tokens, core, 0),
        preferred_element_type=float32,
    ).astype(bf16)
    share = summed_parts(jnp.concatenate([terms, shared_terms], axis=1), "tp_0")
    share = share.reshape(-1, 2 * unit_rows, lanes)
    part = (jax.nn.silu(share[:, :unit_rows]) * share[:, unit_rows:]).astype(bf16)
    hidden = lax.all_gather(part.reshape(-1, lanes), "tp_0")
    hidden = hidden.reshape(chips, -1, unit_rows, lanes)

    results = jnp.einsum(
        "egfr,egfd->egrd",
        hidden[:, :-1].reshape(experts_core, groups, unit_rows, lanes),
        for_groups(down_pair),
        preferred_element_type=float32,
    ).astype(bf16)
    results = results.reshape(experts_core, shards, CAPACITY, 2 * slice_width).transpose(1, 0, 2, 3)
    results = results.reshape(shards, slots, 2 * slice_width)
    total = jnp.einsum("brt,brd->btd", combine, results, preferred_element_type=float32)
    shared_out = jnp.einsum(
        "bft,fd->btd", hidden[:, -1], down_shared_pair, preferred_element_type=float32
    )
    halves = jnp.arange(shards, dtype=jnp.int32)[:, None, None] // (shards // 2) == core
    total = total + jnp.where(halves, jnp.concatenate([shared_out, shared_out]), 0.0)
    total = total[:, :, :slice_width] + swap_cores(
        total[:, :, slice_width:].astype(bf16).reshape(-1, slice_width)
    ).reshape(shards, tok_rows, slice_width).astype(float32)
    served = tie(served, hidden)
    partials = exchange(tie(total.astype(bf16), served), "fs")
    layer_out = jnp.sum(partials.astype(float32), axis=0).astype(bf16)

    served = served.reshape(shards, experts_here + 1, 3, unit_rows, slice_width)
    served = served.transpose(2, 1, 0, 3, 4).reshape(
        3, experts_here + 1, shards * unit_rows, slice_width
    )
    gate_here, up_here, down_here = served[0], served[1], served[2]
    return (
        gate_here[:experts_here],
        up_here[:experts_here],
        down_here[:experts_here],
        gate_here[experts_here],
        up_here[experts_here],
        down_here[experts_here],
        layer_out,
    )


def solution(mesh):
    split = Mesh(
        mesh.devices.reshape(mesh.shape["grp"], mesh.shape["fs"], mesh.shape["tp"] // 2, 2),
        ("grp", "fs", "tp_0", "tp_1"),
    )
    return jax.shard_map(
        layer,
        mesh=split,
        in_specs=(
            P(("grp", "fs"), TP),
            P(TP),
            P(("grp", "fs"), None),
            P(("grp", "fs"), None),
            P(None, "fs", TP),
            P(None, "fs", TP),
            P(None, "fs", TP),
            P("fs", TP),
            P("fs", TP),
            P("fs", TP),
        ),
        out_specs=(
            P(("grp", "fs"), None, TP),
            P(("grp", "fs"), None, TP),
            P(("grp", "fs"), None, TP),
            P("grp", TP),
            P("grp", TP),
            P("grp", TP),
            P(("grp", "fs"), TP),
        ),
        check_vma=False,
    )
```

profile of v0, /device:TPU:80, one launch (start us, length us, event | category | flops | bytes accessed | tf_op | source)
XLA Modules:
  0.0 248.0 jit_solution(16299472129079495663)
XLA Ops:
  0.7 0.9 convert_reduce_fusion
  2.3 7.6 %all-to-all-start = ((f32[16,2,128]{2,1,0:T(2,128)}), f32[16,2,128]{2,1,0:T(2,128)S(1)}, u32[]{:S(2)}, u32[]{:S(2)}) async-start(f32[16,2,128]{2,1,0:T(2,128)} %broadcast_in_dim.51), calls=%async_computation | async-start | bytes 32768 | tf_op jit(solution)/shard_map/all_to_all | solution.py:17
  12.0 5.3 %all-to-all-done = f32[16,2,128]{2,1,0:T(2,128)S(1)} async-done(((f32[16,2,128]{2,1,0:T(2,128)}), f32[16,2,128]{2,1,0:T(2,128)S(1)}, u32[]{:S(2)}, u32[]{:S(2)}) %all-to-all-start) | async-done | bytes 16416 | tf_op jit(solution)/shard_map/all_to_all | solution.py:17
  17.4 0.9 fusion.36
  18.2 0.9 broadcast_in_dim.52
  19.1 43.7 %all-to-all-start.1 = ((bf16[16,144,128]{2,1,0:T(8,128)(2,1)}), bf16[16,144,128]{2,1,0:T(8,128)(2,1)}, u32[]{:S(2)}, u32[]{:S(2)}) async-start(bf16[16,144,128]{2,1,0:T(8,128)(2,1)} %broadcast_in_dim.52), calls=%async_computation.1 | async-start | bytes 1179648 | tf_op jit(solution)/shard_map/all_to_all | solution.py:17
  64.1 1.5 multiply_convert_fusion.1
  65.7 1.5 pad_maximum_fusion
  67.2 26.5 %all-to-all-done.1 = bf16[16,144,128]{2,1,0:T(8,128)(2,1)} async-done(((bf16[16,144,128]{2,1,0:T(8,128)(2,1)}), bf16[16,144,128]{2,1,0:T(8,128)(2,1)}, u32[]{:S(2)}, u32[]{:S(2)}) %all-to-all-start.1) | async-done | bytes 589856 | tf_op jit(solution)/shard_map/all_to_all | solution.py:17
  93.7 7.7 %all-to-all-start.2 = ((bf16[16,5,96,128]{3,2,1,0:T(8,128)(2,1)}), bf16[16,5,96,128]{3,2,1,0:T(8,128)(2,1)S(1)}, u32[]{:S(2)}, u32[]{:S(2)}) async-start(bf16[16,5,96,128]{3,2,1,0:T(8,128)(2,1)} %pad_maximum_fusion), calls=%async_computation.2 | async-start | bytes 3932160 | tf_op jit(solution)/shard_map/all_to_all | solution.py:17
  101.5 1.0 fusion.11
  102.4 0.8 maximum_maximum_fusion
  103.3 1.9 collective-permute-start
  105.3 2.6 %collective-permute-start.1 = (bf16[1056,128]{1,0:T(8,128)(2,1)S(1)}, bf16[1056,128]{1,0:T(8,128)(2,1)S(1)}, u32[]{:S(2)}, u32[]{:S(2)}) collective-permute-start(bf16[1056,128]{1,0:T(8,128)(2,1)S(1)} %bitcast.119), channel_id=1, source_target_pairs={{0,1},{1,0},{2,3},{3,2},{4,5},{5,4},{6,7},{7,6},{8,9},{9,8},{10,11... | collective-permute-start | bytes 811016 | tf_op jit(solution)/shard_map/ppermute | solution.py:42
  108.1 0.9 collective-permute-done.1
  109.1 0.9 pad_maximum_fusion.5
  110.0 1.1 slice.114
  111.9 1.1 slice.97
  113.0 2.3 collective-permute-start.2
  115.3 1.4 slice_convert_fusion.1
  117.6 1.0 bitcast_compare_fusion
  118.7 1.8 convolution_convert_fusion.1
  121.6 2.3 convolution_convert_fusion.2
  123.9 1.1 fusion.32
  125.0 2.6 %collective-permute-start.3 = (bf16[832,128]{1,0:T(8,128)(2,1)}, bf16[832,128]{1,0:T(8,128)(2,1)}, u32[]{:S(2)}, u32[]{:S(2)}) collective-permute-start(bf16[832,128]{1,0:T(8,128)(2,1)} %get-tuple-element.23), channel_id=1, source_target_pairs={{0,8},{2,10},{4,12},{6,14},{8,0},{10,2},{12,4},{14,6},{1,9},{3,11}... | collective-permute-start | bytes 638984 | tf_op jit(solution)/shard_map/ppermute | solution.py:22
  127.6 5.1 %collective-permute-start.4 = (bf16[832,128]{1,0:T(8,128)(2,1)}, bf16[832,128]{1,0:T(8,128)(2,1)}, u32[]{:S(2)}, u32[]{:S(2)}) collective-permute-start(bf16[832,128]{1,0:T(8,128)(2,1)} %get-tuple-element.24), channel_id=1, source_target_pairs={{0,6},{2,8},{4,10},{6,12},{8,14},{10,0},{12,2},{14,4},{1,7},{3,9},... | collective-permute-start | bytes 638984 | tf_op jit(solution)/shard_map/ppermute | solution.py:22
  132.7 3.8 %collective-permute-start.5 = (bf16[832,128]{1,0:T(8,128)(2,1)}, bf16[832,128]{1,0:T(8,128)(2,1)}, u32[]{:S(2)}, u32[]{:S(2)}) collective-permute-start(bf16[832,128]{1,0:T(8,128)(2,1)} %get-tuple-element.25), channel_id=1, source_target_pairs={{0,10},{2,12},{4,14},{6,0},{8,2},{10,4},{12,6},{14,8},{1,11},{3,13... | collective-permute-start | bytes 638984 | tf_op jit(solution)/shard_map/ppermute | solution.py:22
  136.5 4.2 %collective-permute-start.6 = (bf16[832,128]{1,0:T(8,128)(2,1)}, bf16[832,128]{1,0:T(8,128)(2,1)}, u32[]{:S(2)}, u32[]{:S(2)}) collective-permute-start(bf16[832,128]{1,0:T(8,128)(2,1)} %get-tuple-element.26), channel_id=1, source_target_pairs={{0,4},{2,6},{4,8},{6,10},{8,12},{10,14},{12,0},{14,2},{1,5},{3,7},... | collective-permute-start | bytes 638984 | tf_op jit(solution)/shard_map/ppermute | solution.py:22
  140.7 3.8 %collective-permute-start.7 = (bf16[832,128]{1,0:T(8,128)(2,1)}, bf16[832,128]{1,0:T(8,128)(2,1)}, u32[]{:S(2)}, u32[]{:S(2)}) collective-permute-start(bf16[832,128]{1,0:T(8,128)(2,1)} %get-tuple-element.27), channel_id=1, source_target_pairs={{0,12},{2,14},{4,0},{6,2},{8,4},{10,6},{12,8},{14,10},{1,13},{3,15... | collective-permute-start | bytes 638984 | tf_op jit(solution)/shard_map/ppermute | solution.py:22
  144.6 1.4 fusion.33
  146.7 2.6 %collective-permute-start.8 = (bf16[832,128]{1,0:T(8,128)(2,1)}, bf16[832,128]{1,0:T(8,128)(2,1)}, u32[]{:S(2)}, u32[]{:S(2)}) collective-permute-start(bf16[832,128]{1,0:T(8,128)(2,1)} %get-tuple-element.28), channel_id=1, source_target_pairs={{0,2},{2,4},{4,6},{6,8},{8,10},{10,12},{12,14},{14,0},{1,3},{3,5},... | collective-permute-start | bytes 638984 | tf_op jit(solution)/shard_map/ppermute | solution.py:22
  149.3 7.8 %collective-permute-done.4 = bf16[832,128]{1,0:T(8,128)(2,1)} collective-permute-done((bf16[832,128]{1,0:T(8,128)(2,1)}, bf16[832,128]{1,0:T(8,128)(2,1)}, u32[]{:S(2)}, u32[]{:S(2)}) %collective-permute-start.4) | collective-permute-done | bytes 213024 | tf_op jit(solution)/shard_map/ppermute | solution.py:22
  157.1 2.8 %collective-permute-start.9 = (bf16[832,128]{1,0:T(8,128)(2,1)}, bf16[832,128]{1,0:T(8,128)(2,1)}, u32[]{:S(2)}, u32[]{:S(2)}) collective-permute-start(bf16[832,128]{1,0:T(8,128)(2,1)} %fusion.33), channel_id=1, source_target_pairs={{0,14},{2,0},{4,2},{6,4},{8,6},{10,8},{12,10},{14,12},{1,15},{3,1}... | collective-permute-start | bytes 638984 | tf_op jit(solution)/shard_map/ppermute | solution.py:22
  160.4 1.2 fusion.1
  161.7 1.9 fusion
  164.3 4.3 %collective-permute-done.8 = bf16[832,128]{1,0:T(8,128)(2,1)} collective-permute-done((bf16[832,128]{1,0:T(8,128)(2,1)}, bf16[832,128]{1,0:T(8,128)(2,1)}, u32[]{:S(2)}, u32[]{:S(2)}) %collective-permute-start.8) | collective-permute-done | bytes 213024 | tf_op jit(solution)/shard_map/ppermute | solution.py:22
  168.6 1.7 fusion.17
  170.3 26.7 %all_gather.3 = bf16[8,416,128]{2,1,0:T(8,128)(2,1)S(1)} all-gather(bf16[1,416,128]{2,1,0:T(8,128)(2,1)S(1)} %bitcast.118), channel_id=1, replica_groups=mesh['grp'=2,'fs'=16,'tp_0'=8,'tp_1'=2] {'tp_0'}, dimensions={0}, use_global_device_ids=true | all-gather | bytes 958464 | tf_op jit(solution)/shard_map/all_gather | solution.py:173
  197.1 1.8 convolution_convert_fusion
  200.0 1.4 fusion.2
  201.5 2.0 collective-permute-start.10
  203.4 1.9 collective-permute-done.10
  205.3 1.0 fusion.6
  206.3 12.0 %all-to-all-start.3 = ((bf16[16,128,128]{2,1,0:T(8,128)(2,1)}), bf16[16,128,128]{2,1,0:T(8,128)(2,1)S(1)}, u32[]{:S(2)}, u32[]{:S(2)}) async-start(bf16[16,128,128]{2,1,0:T(8,128)(2,1)} %fusion.6), calls=%async_computation.3 | async-start | bytes 1048576 | tf_op jit(solution)/shard_map/all_to_all | solution.py:17
  218.7 0.8 copy.49
  219.6 0.8 copy.50
  220.4 0.8 copy.51
  222.0 25.3 %all-to-all-done.3 = bf16[16,128,128]{2,1,0:T(8,128)(2,1)S(1)} async-done(((bf16[16,128,128]{2,1,0:T(8,128)(2,1)}), bf16[16,128,128]{2,1,0:T(8,128)(2,1)S(1)}, u32[]{:S(2)}, u32[]{:S(2)}) %all-to-all-start.3) | async-done | bytes 524320 | tf_op jit(solution)/shard_map/all_to_all | solution.py:17
  (95 shorter events, 12.1 us)
Async XLA Ops:
  0.6 62.2 %copy-start.5 = (f32[64,32,128]{2,1,0:T(8,128)S(1)}, f32[64,32,128]{2,1,0:T(8,128)}, u32[]{:S(2)}) copy-start(f32[64,32,128]{2,1,0:T(8,128)} %param.16) | copy-start | bytes 3145732
  0.6 62.3 %copy-start.14 = (f32[32,128]{1,0:T(8,128)S(1)}, f32[32,128]{1,0:T(8,128)}, u32[]{:S(2)}) copy-start(f32[32,128]{1,0:T(8,128)} %param.19) | copy-start | bytes 49156
  0.7 62.3 %copy-start.22 = (f32[128]{0:T(128)S(1)}, f32[128]{0:T(128)}, u32[]{:S(2)}) copy-start(f32[128]{0:T(128)} %param.11) | copy-start | bytes 1540
  0.7 62.3 %copy-start.18 = (f32[32,128]{1,0:T(8,128)S(1)}, f32[32,128]{1,0:T(8,128)}, u32[]{:S(2)}) copy-start(f32[32,128]{1,0:T(8,128)} %param.17) | copy-start | bytes 49156
  0.7 62.3 %copy-start.19 = (f32[32,128]{1,0:T(8,128)S(1)}, f32[32,128]{1,0:T(8,128)}, u32[]{:S(2)}) copy-start(f32[32,128]{1,0:T(8,128)} %param.18) | copy-start | bytes 49156
  2.3 15.1 %all-to-all-start = ((f32[16,2,128]{2,1,0:T(2,128)}), f32[16,2,128]{2,1,0:T(2,128)S(1)}, u32[]{:S(2)}, u32[]{:S(2)}) async-start(f32[16,2,128]{2,1,0:T(2,128)} %broadcast_in_dim.51), calls=%async_computation | async-start | bytes 32768 | tf_op jit(solution)/shard_map/all_to_all | solution.py:17
  19.1 74.6 %all-to-all-start.1 = ((bf16[16,144,128]{2,1,0:T(8,128)(2,1)}), bf16[16,144,128]{2,1,0:T(8,128)(2,1)}, u32[]{:S(2)}, u32[]{:S(2)}) async-start(bf16[16,144,128]{2,1,0:T(8,128)(2,1)} %broadcast_in_dim.52), calls=%async_computation.1 | async-start | bytes 1179648 | tf_op jit(solution)/shard_map/all_to_all | solution.py:17
  62.8 1.2 copy-start.6
  63.0 0.6 copy-start.11
  63.0 39.4 %copy-start.9 = (bf16[32,128]{1,0:T(8,128)(2,1)}, bf16[32,128]{1,0:T(8,128)(2,1)S(1)}, u32[]{:S(2)}) copy-start(bf16[32,128]{1,0:T(8,128)(2,1)S(1)} %get-tuple-element.37) | copy-start | bytes 24580
  93.7 112.6 %all-to-all-start.2 = ((bf16[16,5,96,128]{3,2,1,0:T(8,128)(2,1)}), bf16[16,5,96,128]{3,2,1,0:T(8,128)(2,1)S(1)}, u32[]{:S(2)}, u32[]{:S(2)}) async-start(bf16[16,5,96,128]{3,2,1,0:T(8,128)(2,1)} %pad_maximum_fusion), calls=%async_computation.2 | async-start | bytes 3932160 | tf_op jit(solution)/shard_map/all_to_all | solution.py:17
  101.4 1.0 copy-start.12
  101.4 3.8 %copy-start.15 = (f32[32,128]{1,0:T(8,128)S(1)}, f32[32,128]{1,0:T(8,128)}, u32[]{:S(2)}) copy-start(f32[32,128]{1,0:T(8,128)} %param.19) | copy-start | bytes 49156
  103.3 6.7 %collective-permute-start = (bf16[2112,128]{1,0:T(8,128)(2,1)}, bf16[2112,128]{1,0:T(8,128)(2,1)}, u32[]{:S(2)}, u32[]{:S(2)}) collective-permute-start(bf16[2112,128]{1,0:T(8,128)(2,1)} %bitcast.9), channel_id=1, source_target_pairs={{0,1},{1,0},{2,3},{3,2},{4,5},{5,4},{6,7},{7,6},{8,9},{9,8},{10,11... | collective-permute-start | bytes 1622024 | tf_op jit(solution)/shard_map/ppermute | solution.py:42
  105.2 6.5 %copy-start.1 = (bf16[32,64,128]{2,1,0:T(8,128)(2,1)S(1)}, bf16[32,64,128]{2,1,0:T(8,128)(2,1)}, u32[]{:S(2)}) copy-start(bf16[32,64,128]{2,1,0:T(8,128)(2,1)} %get-tuple-element.29) | copy-start | bytes 1572868
  105.3 3.7 %collective-permute-start.1 = (bf16[1056,128]{1,0:T(8,128)(2,1)S(1)}, bf16[1056,128]{1,0:T(8,128)(2,1)S(1)}, u32[]{:S(2)}, u32[]{:S(2)}) collective-permute-start(bf16[1056,128]{1,0:T(8,128)(2,1)S(1)} %bitcast.119), channel_id=1, source_target_pairs={{0,1},{1,0},{2,3},{3,2},{4,5},{5,4},{6,7},{7,6},{8,9},{9,8},{10,11... | collective-permute-start | bytes 811016 | tf_op jit(solution)/shard_map/ppermute | solution.py:42
  108.1 9.5 %copy-start.16 = (s32[768]{0:T(1024)}, s32[768]{0:T(1024)S(1)}, u32[]{:S(2)}) copy-start(s32[768]{0:T(1024)S(1)} %eq.60) | copy-start | bytes 9220
  108.1 8.6 %copy-start.20 = (s32[32]{0:T(128)}, s32[32]{0:T(128)S(1)}, u32[]{:S(2)}) copy-start(s32[32]{0:T(128)S(1)} %iota_add_fusion) | copy-start | bytes 388
  109.0 2.9 %copy-start.8 = (bf16[1056,128]{1,0:T(8,128)(2,1)}, bf16[1056,128]{1,0:T(8,128)(2,1)S(1)}, u32[]{:S(2)}) copy-start(bf16[1056,128]{1,0:T(8,128)(2,1)S(1)} %collective-permute-done.1) | copy-start | bytes 811012
  113.0 5.6 %collective-permute-start.2 = (bf16[16,128,128]{2,1,0:T(8,128)(2,1)S(1)}, bf16[16,128,128]{2,1,0:T(8,128)(2,1)S(1)}, u32[]{:S(2)}, u32[]{:S(2)}) collective-permute-start(bf16[16,128,128]{2,1,0:T(8,128)(2,1)S(1)} %slice.97), channel_id=1, source_target_pairs={{0,1},{1,0},{2,3},{3,2},{4,5},{5,4},{6,7},{7,6},{8,9},{9,8},{10,11... | collective-permute-start | bytes 1572872 | tf_op jit(solution)/shard_map/ppermute | solution.py:42
  116.8 0.6 copy-start.7
  117.6 1.1 copy-start
  120.4 0.8 copy-start.10
  120.4 0.8 copy-start.13
  121.5 2.3 copy-start.3
  123.9 36.6 %copy-start.21 = (s32[32]{0:T(128)S(1)}, s32[32]{0:T(128)}, u32[]{:S(2)}) copy-start(s32[32]{0:T(128)} %copy-done.20) | copy-start | bytes 388
  123.9 37.8 %copy-start.17 = (s32[768]{0:T(1024)S(1)}, s32[768]{0:T(1024)}, u32[]{:S(2)}) copy-start(s32[768]{0:T(1024)} %copy-done.16) | copy-start | bytes 9220
  125.0 21.7 %collective-permute-start.3 = (bf16[832,128]{1,0:T(8,128)(2,1)}, bf16[832,128]{1,0:T(8,128)(2,1)}, u32[]{:S(2)}, u32[]{:S(2)}) collective-permute-start(bf16[832,128]{1,0:T(8,128)(2,1)} %get-tuple-element.23), channel_id=1, source_target_pairs={{0,8},{2,10},{4,12},{6,14},{8,0},{10,2},{12,4},{14,6},{1,9},{3,11}... | collective-permute-start | bytes 638984 | tf_op jit(solution)/shard_map/ppermute | solution.py:22
  127.6 29.5 %collective-permute-start.4 = (bf16[832,128]{1,0:T(8,128)(2,1)}, bf16[832,128]{1,0:T(8,128)(2,1)}, u32[]{:S(2)}, u32[]{:S(2)}) collective-permute-start(bf16[832,128]{1,0:T(8,128)(2,1)} %get-tuple-element.24), channel_id=1, source_target_pairs={{0,6},{2,8},{4,10},{6,12},{8,14},{10,0},{12,2},{14,4},{1,7},{3,9},... | collective-permute-start | bytes 638984 | tf_op jit(solution)/shard_map/ppermute | solution.py:22
  132.7 30.9 %collective-permute-start.5 = (bf16[832,128]{1,0:T(8,128)(2,1)}, bf16[832,128]{1,0:T(8,128)(2,1)}, u32[]{:S(2)}, u32[]{:S(2)}) collective-permute-start(bf16[832,128]{1,0:T(8,128)(2,1)} %get-tuple-element.25), channel_id=1, source_target_pairs={{0,10},{2,12},{4,14},{6,0},{8,2},{10,4},{12,6},{14,8},{1,11},{3,13... | collective-permute-start | bytes 638984 | tf_op jit(solution)/shard_map/ppermute | solution.py:22
  136.5 27.1 %collective-permute-start.6 = (bf16[832,128]{1,0:T(8,128)(2,1)}, bf16[832,128]{1,0:T(8,128)(2,1)}, u32[]{:S(2)}, u32[]{:S(2)}) collective-permute-start(bf16[832,128]{1,0:T(8,128)(2,1)} %get-tuple-element.26), channel_id=1, source_target_pairs={{0,4},{2,6},{4,8},{6,10},{8,12},{10,14},{12,0},{14,2},{1,5},{3,7},... | collective-permute-start | bytes 638984 | tf_op jit(solution)/shard_map/ppermute | solution.py:22
  140.7 23.6 %collective-permute-start.7 = (bf16[832,128]{1,0:T(8,128)(2,1)}, bf16[832,128]{1,0:T(8,128)(2,1)}, u32[]{:S(2)}, u32[]{:S(2)}) collective-permute-start(bf16[832,128]{1,0:T(8,128)(2,1)} %get-tuple-element.27), channel_id=1, source_target_pairs={{0,12},{2,14},{4,0},{6,2},{8,4},{10,6},{12,8},{14,10},{1,13},{3,15... | collective-permute-start | bytes 638984 | tf_op jit(solution)/shard_map/ppermute | solution.py:22
  146.7 21.9 %collective-permute-start.8 = (bf16[832,128]{1,0:T(8,128)(2,1)}, bf16[832,128]{1,0:T(8,128)(2,1)}, u32[]{:S(2)}, u32[]{:S(2)}) collective-permute-start(bf16[832,128]{1,0:T(8,128)(2,1)} %get-tuple-element.28), channel_id=1, source_target_pairs={{0,2},{2,4},{4,6},{6,8},{8,10},{10,12},{12,14},{14,0},{1,3},{3,5},... | collective-permute-start | bytes 638984 | tf_op jit(solution)/shard_map/ppermute | solution.py:22
  157.1 11.5 %collective-permute-start.9 = (bf16[832,128]{1,0:T(8,128)(2,1)}, bf16[832,128]{1,0:T(8,128)(2,1)}, u32[]{:S(2)}, u32[]{:S(2)}) collective-permute-start(bf16[832,128]{1,0:T(8,128)(2,1)} %fusion.33), channel_id=1, source_target_pairs={{0,14},{2,0},{4,2},{6,4},{8,6},{10,8},{12,10},{14,12},{1,15},{3,1}... | collective-permute-start | bytes 638984 | tf_op jit(solution)/shard_map/ppermute | solution.py:22
  160.4 8.2 %copy-start.4 = (bf16[8,64,128]{2,1,0:T(8,128)(2,1)S(1)}, bf16[8,64,128]{2,1,0:T(8,128)(2,1)}, u32[]{:S(2)}) copy-start(bf16[8,64,128]{2,1,0:T(8,128)(2,1)} %copy-done.3) | copy-start | bytes 393220
  170.3 26.8 %copy-start.2 = (bf16[32,32,256]{2,1,0:T(8,128)(2,1)S(1)}, bf16[32,32,256]{2,1,0:T(8,128)(2,1)}, u32[]{:S(2)}) copy-start(bf16[32,32,256]{2,1,0:T(8,128)(2,1)} %pad_maximum_fusion.5) | copy-start | bytes 1572868
  198.9 0.7 slice-start
  198.9 1.0 copy-start.23
  201.5 3.8 %collective-permute-start.10 = (bf16[2048,128]{1,0:T(8,128)(2,1)S(1)}, bf16[2048,128]{1,0:T(8,128)(2,1)S(1)}, u32[]{:S(2)}, u32[]{:S(2)}) collective-permute-start(bf16[2048,128]{1,0:T(8,128)(2,1)S(1)} %bitcast.116), channel_id=1, source_target_pairs={{0,1},{1,0},{2,3},{3,2},{4,5},{5,4},{6,7},{7,6},{8,9},{9,8},{10,11... | collective-permute-start | bytes 1572872 | tf_op jit(solution)/shard_map/ppermute | solution.py:42
  206.3 41.0 %all-to-all-start.3 = ((bf16[16,128,128]{2,1,0:T(8,128)(2,1)}), bf16[16,128,128]{2,1,0:T(8,128)(2,1)S(1)}, u32[]{:S(2)}, u32[]{:S(2)}) async-start(bf16[16,128,128]{2,1,0:T(8,128)(2,1)} %fusion.6), calls=%async_computation.3 | async-start | bytes 1048576 | tf_op jit(solution)/shard_map/all_to_all | solution.py:17
where the time goes:
time: 249 us; the launch traced here: 248 us
  starting transfers between devices  105 us (42%)
  waiting for transfers between devices  73.4 us (29%)
  blocking collectives  26.7 us (11%)
  other arithmetic  22.4 us (9%)
  local copies, waits for them, and re-layouts  11.2 us (4%)
  matrix products  8.14 us (3%)
    all_to_all x4, starting transfers between devices, exchange(): return lax.all_to_all(array, axis, 0, 0, tiled=True)  71 us
    all_to_all x4, waiting for transfers between devices, exchange(): return lax.all_to_all(array, axis, 0, 0, tiled=True)  57.2 us
    all_gather x1, blocking collectives, layer(): hidden = lax.all_gather(part.reshape(-1, lanes), 'tp_0')  26.7 us
    ppermute x7, starting transfers between devices, rotated(): lax.ppermute(array, axis, [(i, (i + by) % size) for i in range(size)])  25 us
    ppermute x7, waiting for transfers between devices, rotated(): lax.ppermute(array, axis, [(i, (i + by) % size) for i in range(size)])  13.4 us
    ppermute x4, starting transfers between devices, swap_cores(): return lax.ppermute(array, 'tp_1', [(0, 1), (1, 0)])  8.77 us
  transfers between devices with their start and end apart: 15, of which 9 were waited for; matrix products, arithmetic and copies ran while one was open for 15% of the time, Pallas kernels for 0%

commit v1 on v0

--- a/solution.py
+++ b/solution.py
@@ -22,20 +22,26 @@
     return lax.ppermute(array, axis, [(i, (i + by) % size) for i in range(size)])
 
 
-def distances(axis):
-    size = lax.axis_size(axis)
-    return sorted(range(1, size), key=lambda by: -min(by, size - by))
-
-
 def summed_parts(blocks, axis):
     at = lax.axis_index(axis)
     size = lax.axis_size(axis)
+    half_way = size // 2
+    cut = blocks.shape[1] // 2
     pick = lambda i: lax.dynamic_index_in_dim(blocks, i % size, 0, keepdims=False)
-    parts = [rotated(pick(at + by), axis, by) for by in distances(axis)]
-    total = pick(at).astype(jnp.float32)
-    for part in parts:
-        total = total + part.astype(jnp.float32)
-    return total
+    far = pick(at + half_way)
+    first = rotated(jnp.concatenate([pick(at - 1), far[cut:]]), axis, size - 1)
+    total = pick(at).astype(jnp.float32) + first[: -cut].astype(jnp.float32)
+    for by in range(half_way - 1, 1, -1):
+        total = total + rotated(pick(at + by), axis, by).astype(jnp.float32)
+        if by < half_way - 1:
+            total = total + rotated(pick(at - by), axis, size - by).astype(jnp.float32)
+    total = total + rotated(pick(at + 1), axis, 1).astype(jnp.float32)
+    upper = rotated(far[:cut], axis, half_way)
+    last = rotated(
+        jnp.concatenate([pick(at - half_way + 1), first[-cut:]]), axis, size - half_way + 1
+    )
+    total = total + last[: -cut].astype(jnp.float32)
+    return total + jnp.concatenate([upper, last[-cut:]]).astype(jnp.float32)
 
 
 def swap_cores(array):

time: 249 us -> 261 us (1.048)
  waiting for transfers between devices: 73.4 us -> 81.3 us
    ppermute x7, waiting for transfers between devices: 13.4 us -> 21.3 us  [rotated(): lax.ppermute(array, axis, [(i, (i + by) % size) for i in range(size)])]
where the time goes in v1:
time: 261 us; the launch traced here: 260 us
  starting transfers between devices  107 us (41%)
  waiting for transfers between devices  81.3 us (31%)
  blocking collectives  26.6 us (10%)
  other arithmetic  22.9 us (9%)
  local copies, waits for them, and re-layouts  12.7 us (5%)
  matrix products  8.14 us (3%)
    all_to_all x4, starting transfers between devices, exchange(): return lax.all_to_all(array, axis, 0, 0, tiled=True)  71.3 us
    all_to_all x4, waiting for transfers between devices, exchange(): return lax.all_to_all(array, axis, 0, 0, tiled=True)  57.2 us
    all_gather x1, blocking collectives, layer(): hidden = lax.all_gather(part.reshape(-1, lanes), 'tp_0')  26.6 us
    ppermute x7, starting transfers between devices, rotated(): lax.ppermute(array, axis, [(i, (i + by) % size) for i in range(size)])  26.5 us
    ppermute x7, waiting for transfers between devices, rotated(): lax.ppermute(array, axis, [(i, (i + by) % size) for i in range(size)])  21.3 us
    ppermute x4, starting transfers between devices, swap_cores(): return lax.ppermute(array, 'tp_1', [(0, 1), (1, 0)])  8.77 us
  transfers between devices with their start and end apart: 15, of which 9 were waited for; matrix products, arithmetic and copies ran while one was open for 15% of the time, Pallas kernels for 0%

profile of v1, /device:TPU:80, one launch (start us, length us, event | category | flops | bytes accessed | tf_op | source)
XLA Modules:
  0.0 259.7 jit_solution(1083401973202629655)
XLA Ops:
  0.7 0.9 convert_reduce_fusion
  2.3 7.6 %all-to-all-start = ((f32[16,2,128]{2,1,0:T(2,128)}), f32[16,2,128]{2,1,0:T(2,128)S(1)}, u32[]{:S(2)}, u32[]{:S(2)}) async-start(f32[16,2,128]{2,1,0:T(2,128)} %broadcast_in_dim.51), calls=%async_computation | async-start | bytes 32768 | tf_op jit(solution)/shard_map/all_to_all | solution.py:17
  12.0 5.3 %all-to-all-done = f32[16,2,128]{2,1,0:T(2,128)S(1)} async-done(((f32[16,2,128]{2,1,0:T(2,128)}), f32[16,2,128]{2,1,0:T(2,128)S(1)}, u32[]{:S(2)}, u32[]{:S(2)}) %all-to-all-start) | async-done | bytes 16416 | tf_op jit(solution)/shard_map/all_to_all | solution.py:17
  17.4 0.9 fusion.35
  18.2 0.9 broadcast_in_dim.52
  19.1 43.7 %all-to-all-start.1 = ((bf16[16,144,128]{2,1,0:T(8,128)(2,1)}), bf16[16,144,128]{2,1,0:T(8,128)(2,1)}, u32[]{:S(2)}, u32[]{:S(2)}) async-start(bf16[16,144,128]{2,1,0:T(8,128)(2,1)} %broadcast_in_dim.52), calls=%async_computation.1 | async-start | bytes 1179648 | tf_op jit(solution)/shard_map/all_to_all | solution.py:17
  64.1 1.5 multiply_convert_fusion.1
  65.7 1.5 pad_maximum_fusion
  67.2 26.5 %all-to-all-done.1 = bf16[16,144,128]{2,1,0:T(8,128)(2,1)} async-done(((bf16[16,144,128]{2,1,0:T(8,128)(2,1)}), bf16[16,144,128]{2,1,0:T(8,128)(2,1)}, u32[]{:S(2)}, u32[]{:S(2)}) %all-to-all-start.1) | async-done | bytes 589856 | tf_op jit(solution)/shard_map/all_to_all | solution.py:17
  93.7 7.7 %all-to-all-start.2 = ((bf16[16,5,96,128]{3,2,1,0:T(8,128)(2,1)}), bf16[16,5,96,128]{3,2,1,0:T(8,128)(2,1)S(1)}, u32[]{:S(2)}, u32[]{:S(2)}) async-start(bf16[16,5,96,128]{3,2,1,0:T(8,128)(2,1)} %pad_maximum_fusion), calls=%async_computation.2 | async-start | bytes 3932160 | tf_op jit(solution)/shard_map/all_to_all | solution.py:17
  101.5 1.0 fusion.11
  103.3 1.9 collective-permute-start
  105.3 2.6 collective-permute-start.1
  108.2 0.9 collective-permute-done.1
  109.1 0.9 pad_maximum_fusion.5
  110.0 1.1 slice.146
  111.9 1.1 slice.121
  113.0 2.3 collective-permute-start.2
  115.3 1.4 slice_convert_fusion.1
  117.6 1.0 bitcast_compare_fusion
  118.6 1.8 convolution_convert_fusion.1
  121.6 2.3 convolution_convert_fusion.2
  123.9 0.9 fusion.32
  125.4 2.5 collective-permute-start.3
  127.9 9.0 %collective-permute-done.3 = bf16[1248,128]{1,0:T(8,128)(2,1)S(1)} collective-permute-done((bf16[1248,128]{1,0:T(8,128)(2,1)S(1)}, bf16[1248,128]{1,0:T(8,128)(2,1)S(1)}, u32[]{:S(2)}, u32[]{:S(2)}) %collective-permute-start.3) | collective-permute-done | bytes 319520 | tf_op jit(solution)/shard_map/ppermute | solution.py:22
  137.8 2.5 collective-permute-start.8
  140.3 5.2 %collective-permute-start.4 = (bf16[832,128]{1,0:T(8,128)(2,1)}, bf16[832,128]{1,0:T(8,128)(2,1)}, u32[]{:S(2)}, u32[]{:S(2)}) collective-permute-start(bf16[832,128]{1,0:T(8,128)(2,1)} %get-tuple-element.26), channel_id=1, source_target_pairs={{0,6},{2,8},{4,10},{6,12},{8,14},{10,0},{12,2},{14,4},{1,7},{3,9},... | collective-permute-start | bytes 638984 | tf_op jit(solution)/shard_map/ppermute | solution.py:22
  145.5 3.7 %collective-permute-start.5 = (bf16[832,128]{1,0:T(8,128)(2,1)}, bf16[832,128]{1,0:T(8,128)(2,1)}, u32[]{:S(2)}, u32[]{:S(2)}) collective-permute-start(bf16[832,128]{1,0:T(8,128)(2,1)} %get-tuple-element.27), channel_id=1, source_target_pairs={{0,4},{2,6},{4,8},{6,10},{8,12},{10,14},{12,0},{14,2},{1,5},{3,7},... | collective-permute-start | bytes 638984 | tf_op jit(solution)/shard_map/ppermute | solution.py:22
  149.2 4.3 %collective-permute-start.6 = (bf16[832,128]{1,0:T(8,128)(2,1)}, bf16[832,128]{1,0:T(8,128)(2,1)}, u32[]{:S(2)}, u32[]{:S(2)}) collective-permute-start(bf16[832,128]{1,0:T(8,128)(2,1)} %get-tuple-element.28), channel_id=1, source_target_pairs={{0,12},{2,14},{4,0},{6,2},{8,4},{10,6},{12,8},{14,10},{1,13},{3,15... | collective-permute-start | bytes 638984 | tf_op jit(solution)/shard_map/ppermute | solution.py:22
  153.5 1.4 fusion.27
  155.0 3.7 %collective-permute-start.7 = (bf16[832,128]{1,0:T(8,128)(2,1)}, bf16[832,128]{1,0:T(8,128)(2,1)}, u32[]{:S(2)}, u32[]{:S(2)}) collective-permute-start(bf16[832,128]{1,0:T(8,128)(2,1)} %fusion.27), channel_id=1, source_target_pairs={{0,2},{2,4},{4,6},{6,8},{8,10},{10,12},{12,14},{14,0},{1,3},{3,5},... | collective-permute-start | bytes 638984 | tf_op jit(solution)/shard_map/ppermute | solution.py:22
  159.2 6.6 %collective-permute-done.8 = bf16[1248,128]{1,0:T(8,128)(2,1)} collective-permute-done((bf16[1248,128]{1,0:T(8,128)(2,1)}, bf16[1248,128]{1,0:T(8,128)(2,1)}, u32[]{:S(2)}, u32[]{:S(2)}) %collective-permute-start.8) | collective-permute-done | bytes 319520 | tf_op jit(solution)/shard_map/ppermute | solution.py:22
  165.8 4.7 %collective-permute-start.9 = (bf16[416,128]{1,0:T(8,128)(2,1)}, bf16[416,128]{1,0:T(8,128)(2,1)S(1)}, u32[]{:S(2)}, u32[]{:S(2)}) collective-permute-start(bf16[416,128]{1,0:T(8,128)(2,1)} %get-tuple-element.35), channel_id=1, source_target_pairs={{0,8},{2,10},{4,12},{6,14},{8,0},{10,2},{12,4},{14,6},{1,9},{3,11}... | collective-permute-start | bytes 319496 | tf_op jit(solution)/shard_map/ppermute | solution.py:22
  170.4 1.2 fusion.1
  171.6 1.9 fusion
  173.5 0.9 slice.155
  174.4 2.2 collective-permute-done.9
  176.7 3.5 %collective-permute-done.7 = bf16[832,128]{1,0:T(8,128)(2,1)} collective-permute-done((bf16[832,128]{1,0:T(8,128)(2,1)}, bf16[832,128]{1,0:T(8,128)(2,1)}, u32[]{:S(2)}, u32[]{:S(2)}) %collective-permute-start.7) | collective-permute-done | bytes 213024 | tf_op jit(solution)/shard_map/ppermute | solution.py:22
  180.2 1.5 fusion.17
  181.8 26.6 %all_gather.3 = bf16[8,416,128]{2,1,0:T(8,128)(2,1)S(1)} all-gather(bf16[1,416,128]{2,1,0:T(8,128)(2,1)S(1)} %bitcast.120), channel_id=1, replica_groups=mesh['grp'=2,'fs'=16,'tp_0'=8,'tp_1'=2] {'tp_0'}, dimensions={0}, use_global_device_ids=true | all-gather | bytes 958464 | tf_op jit(solution)/shard_map/all_gather | solution.py:179
  208.5 1.8 convolution_convert_fusion
  211.4 1.4 fusion.2
  212.9 2.0 collective-permute-start.10
  214.9 1.9 collective-permute-done.10
  216.7 1.0 fusion.6
  217.7 12.2 %all-to-all-start.3 = ((bf16[16,128,128]{2,1,0:T(8,128)(2,1)}), bf16[16,128,128]{2,1,0:T(8,128)(2,1)S(1)}, u32[]{:S(2)}, u32[]{:S(2)}) async-start(bf16[16,128,128]{2,1,0:T(8,128)(2,1)} %fusion.6), calls=%async_computation.3 | async-start | bytes 1048576 | tf_op jit(solution)/shard_map/all_to_all | solution.py:17
  230.4 0.8 copy.49
  233.6 25.3 %all-to-all-done.3 = bf16[16,128,128]{2,1,0:T(8,128)(2,1)S(1)} async-done(((bf16[16,128,128]{2,1,0:T(8,128)(2,1)}), bf16[16,128,128]{2,1,0:T(8,128)(2,1)S(1)}, u32[]{:S(2)}, u32[]{:S(2)}) %all-to-all-start.3) | async-done | bytes 524320 | tf_op jit(solution)/shard_map/all_to_all | solution.py:17
  (104 shorter events, 14.7 us)
Async XLA Ops:
  0.6 62.2 %copy-start.5 = (f32[64,32,128]{2,1,0:T(8,128)S(1)}, f32[64,32,128]{2,1,0:T(8,128)}, u32[]{:S(2)}) copy-start(f32[64,32,128]{2,1,0:T(8,128)} %param.16) | copy-start | bytes 3145732
  0.6 62.3 %copy-start.16 = (f32[32,128]{1,0:T(8,128)S(1)}, f32[32,128]{1,0:T(8,128)}, u32[]{:S(2)}) copy-start(f32[32,128]{1,0:T(8,128)} %param.19) | copy-start | bytes 49156
  0.7 62.3 %copy-start.24 = (f32[128]{0:T(128)S(1)}, f32[128]{0:T(128)}, u32[]{:S(2)}) copy-start(f32[128]{0:T(128)} %param.11) | copy-start | bytes 1540
  0.7 62.3 %copy-start.20 = (f32[32,128]{1,0:T(8,128)S(1)}, f32[32,128]{1,0:T(8,128)}, u32[]{:S(2)}) copy-start(f32[32,128]{1,0:T(8,128)} %param.17) | copy-start | bytes 49156
  0.7 62.3 %copy-start.21 = (f32[32,128]{1,0:T(8,128)S(1)}, f32[32,128]{1,0:T(8,128)}, u32[]{:S(2)}) copy-start(f32[32,128]{1,0:T(8,128)} %param.18) | copy-start | bytes 49156
  2.3 15.1 %all-to-all-start = ((f32[16,2,128]{2,1,0:T(2,128)}), f32[16,2,128]{2,1,0:T(2,128)S(1)}, u32[]{:S(2)}, u32[]{:S(2)}) async-start(f32[16,2,128]{2,1,0:T(2,128)} %broadcast_in_dim.51), calls=%async_computation | async-start | bytes 32768 | tf_op jit(solution)/shard_map/all_to_all | solution.py:17
  19.1 74.6 %all-to-all-start.1 = ((bf16[16,144,128]{2,1,0:T(8,128)(2,1)}), bf16[16,144,128]{2,1,0:T(8,128)(2,1)}, u32[]{:S(2)}, u32[]{:S(2)}) async-start(bf16[16,144,128]{2,1,0:T(8,128)(2,1)} %broadcast_in_dim.52), calls=%async_computation.1 | async-start | bytes 1179648 | tf_op jit(solution)/shard_map/all_to_all | solution.py:17
  62.8 1.2 copy-start.6
  63.0 0.6 copy-start.13
  63.0 39.4 %copy-start.11 = (bf16[32,128]{1,0:T(8,128)(2,1)}, bf16[32,128]{1,0:T(8,128)(2,1)S(1)}, u32[]{:S(2)}) copy-start(bf16[32,128]{1,0:T(8,128)(2,1)S(1)} %get-tuple-element.39) | copy-start | bytes 24580
  93.7 124.0 %all-to-all-start.2 = ((bf16[16,5,96,128]{3,2,1,0:T(8,128)(2,1)}), bf16[16,5,96,128]{3,2,1,0:T(8,128)(2,1)S(1)}, u32[]{:S(2)}, u32[]{:S(2)}) async-start(bf16[16,5,96,128]{3,2,1,0:T(8,128)(2,1)} %pad_maximum_fusion), calls=%async_computation.2 | async-start | bytes 3932160 | tf_op jit(solution)/shard_map/all_to_all | solution.py:17
  101.4 1.0 copy-start.14
  101.4 3.8 %copy-start.17 = (f32[32,128]{1,0:T(8,128)S(1)}, f32[32,128]{1,0:T(8,128)}, u32[]{:S(2)}) copy-start(f32[32,128]{1,0:T(8,128)} %param.19) | copy-start | bytes 49156
  103.3 6.7 %collective-permute-start = (bf16[2112,128]{1,0:T(8,128)(2,1)}, bf16[2112,128]{1,0:T(8,128)(2,1)}, u32[]{:S(2)}, u32[]{:S(2)}) collective-permute-start(bf16[2112,128]{1,0:T(8,128)(2,1)} %bitcast.9), channel_id=1, source_target_pairs={{0,1},{1,0},{2,3},{3,2},{4,5},{5,4},{6,7},{7,6},{8,9},{9,8},{10,11... | collective-permute-start | bytes 1622024 | tf_op jit(solution)/shard_map/ppermute | solution.py:48
  105.2 6.5 %copy-start.1 = (bf16[32,64,128]{2,1,0:T(8,128)(2,1)S(1)}, bf16[32,64,128]{2,1,0:T(8,128)(2,1)}, u32[]{:S(2)}) copy-start(bf16[32,64,128]{2,1,0:T(8,128)(2,1)} %get-tuple-element.29) | copy-start | bytes 1572868
  105.3 3.7 %collective-permute-start.1 = (bf16[1056,128]{1,0:T(8,128)(2,1)S(1)}, bf16[1056,128]{1,0:T(8,128)(2,1)S(1)}, u32[]{:S(2)}, u32[]{:S(2)}) collective-permute-start(bf16[1056,128]{1,0:T(8,128)(2,1)S(1)} %bitcast.121), channel_id=1, source_target_pairs={{0,1},{1,0},{2,3},{3,2},{4,5},{5,4},{6,7},{7,6},{8,9},{9,8},{10,11... | collective-permute-start | bytes 811016 | tf_op jit(solution)/shard_map/ppermute | solution.py:48
  108.1 9.5 %copy-start.18 = (s32[768]{0:T(1024)}, s32[768]{0:T(1024)S(1)}, u32[]{:S(2)}) copy-start(s32[768]{0:T(1024)S(1)} %eq.60) | copy-start | bytes 9220
  108.2 8.6 %copy-start.22 = (s32[32]{0:T(128)}, s32[32]{0:T(128)S(1)}, u32[]{:S(2)}) copy-start(s32[32]{0:T(128)S(1)} %iota_add_fusion) | copy-start | bytes 388
  109.1 2.9 %copy-start.10 = (bf16[1056,128]{1,0:T(8,128)(2,1)}, bf16[1056,128]{1,0:T(8,128)(2,1)S(1)}, u32[]{:S(2)}) copy-start(bf16[1056,128]{1,0:T(8,128)(2,1)S(1)} %collective-permute-done.1) | copy-start | bytes 811012
  113.0 5.6 %collective-permute-start.2 = (bf16[16,128,128]{2,1,0:T(8,128)(2,1)S(1)}, bf16[16,128,128]{2,1,0:T(8,128)(2,1)S(1)}, u32[]{:S(2)}, u32[]{:S(2)}) collective-permute-start(bf16[16,128,128]{2,1,0:T(8,128)(2,1)S(1)} %slice.121), channel_id=1, source_target_pairs={{0,1},{1,0},{2,3},{3,2},{4,5},{5,4},{6,7},{7,6},{8,9},{9,8},{10,11... | collective-permute-start | bytes 1572872 | tf_op jit(solution)/shard_map/ppermute | solution.py:48
  116.8 0.6 copy-start.7
  117.6 1.0 copy-start
  120.4 0.8 copy-start.12
  120.4 0.8 copy-start.15
  121.5 2.3 copy-start.3
  124.8 45.7 %copy-start.23 = (s32[32]{0:T(128)S(1)}, s32[32]{0:T(128)}, u32[]{:S(2)}) copy-start(s32[32]{0:T(128)} %copy-done.22) | copy-start | bytes 388
  124.8 46.9 %copy-start.19 = (s32[768]{0:T(1024)S(1)}, s32[768]{0:T(1024)}, u32[]{:S(2)}) copy-start(s32[768]{0:T(1024)} %copy-done.18) | copy-start | bytes 9220
  125.4 11.5 %collective-permute-start.3 = (bf16[1248,128]{1,0:T(8,128)(2,1)S(1)}, bf16[1248,128]{1,0:T(8,128)(2,1)S(1)}, u32[]{:S(2)}, u32[]{:S(2)}) collective-permute-start(bf16[1248,128]{1,0:T(8,128)(2,1)S(1)} %pad_maximum_fusion.6), channel_id=1, source_target_pairs={{0,14},{2,0},{4,2},{6,4},{8,6},{10,8},{12,10},{14,12},{1,15},{3,1}... | collective-permute-start | bytes 958472 | tf_op jit(solution)/shard_map/ppermute | solution.py:22
  136.9 0.8 copy-start.8
  137.8 28.0 %collective-permute-start.8 = (bf16[1248,128]{1,0:T(8,128)(2,1)}, bf16[1248,128]{1,0:T(8,128)(2,1)}, u32[]{:S(2)}, u32[]{:S(2)}) collective-permute-start(bf16[1248,128]{1,0:T(8,128)(2,1)} %pad_maximum_fusion.7), channel_id=1, source_target_pairs={{0,10},{2,12},{4,14},{6,0},{8,2},{10,4},{12,6},{14,8},{1,11},{3,13... | collective-permute-start | bytes 958472 | tf_op jit(solution)/shard_map/ppermute | solution.py:22
  140.3 36.4 %collective-permute-start.4 = (bf16[832,128]{1,0:T(8,128)(2,1)}, bf16[832,128]{1,0:T(8,128)(2,1)}, u32[]{:S(2)}, u32[]{:S(2)}) collective-permute-start(bf16[832,128]{1,0:T(8,128)(2,1)} %get-tuple-element.26), channel_id=1, source_target_pairs={{0,6},{2,8},{4,10},{6,12},{8,14},{10,0},{12,2},{14,4},{1,7},{3,9},... | collective-permute-start | bytes 638984 | tf_op jit(solution)/shard_map/ppermute | solution.py:22
  145.5 31.2 %collective-permute-start.5 = (bf16[832,128]{1,0:T(8,128)(2,1)}, bf16[832,128]{1,0:T(8,128)(2,1)}, u32[]{:S(2)}, u32[]{:S(2)}) collective-permute-start(bf16[832,128]{1,0:T(8,128)(2,1)} %get-tuple-element.27), channel_id=1, source_target_pairs={{0,4},{2,6},{4,8},{6,10},{8,12},{10,14},{12,0},{14,2},{1,5},{3,7},... | collective-permute-start | bytes 638984 | tf_op jit(solution)/shard_map/ppermute | solution.py:22
  149.2 27.4 %collective-permute-start.6 = (bf16[832,128]{1,0:T(8,128)(2,1)}, bf16[832,128]{1,0:T(8,128)(2,1)}, u32[]{:S(2)}, u32[]{:S(2)}) collective-permute-start(bf16[832,128]{1,0:T(8,128)(2,1)} %get-tuple-element.28), channel_id=1, source_target_pairs={{0,12},{2,14},{4,0},{6,2},{8,4},{10,6},{12,8},{14,10},{1,13},{3,15... | collective-permute-start | bytes 638984 | tf_op jit(solution)/shard_map/ppermute | solution.py:22
  155.0 25.2 %collective-permute-start.7 = (bf16[832,128]{1,0:T(8,128)(2,1)}, bf16[832,128]{1,0:T(8,128)(2,1)}, u32[]{:S(2)}, u32[]{:S(2)}) collective-permute-start(bf16[832,128]{1,0:T(8,128)(2,1)} %fusion.27), channel_id=1, source_target_pairs={{0,2},{2,4},{4,6},{6,8},{8,10},{10,12},{12,14},{14,0},{1,3},{3,5},... | collective-permute-start | bytes 638984 | tf_op jit(solution)/shard_map/ppermute | solution.py:22
  159.2 21.0 %copy-start.4 = (bf16[8,64,128]{2,1,0:T(8,128)(2,1)S(1)}, bf16[8,64,128]{2,1,0:T(8,128)(2,1)}, u32[]{:S(2)}) copy-start(bf16[8,64,128]{2,1,0:T(8,128)(2,1)} %copy-done.3) | copy-start | bytes 393220
  159.2 21.0 %copy-start.9 = (bf16[1248,128]{1,0:T(8,128)(2,1)S(1)}, bf16[1248,128]{1,0:T(8,128)(2,1)}, u32[]{:S(2)}) copy-start(bf16[1248,128]{1,0:T(8,128)(2,1)} %copy-done.8) | copy-start | bytes 958468
  165.8 10.9 %collective-permute-start.9 = (bf16[416,128]{1,0:T(8,128)(2,1)}, bf16[416,128]{1,0:T(8,128)(2,1)S(1)}, u32[]{:S(2)}, u32[]{:S(2)}) collective-permute-start(bf16[416,128]{1,0:T(8,128)(2,1)} %get-tuple-element.35), channel_id=1, source_target_pairs={{0,8},{2,10},{4,12},{6,14},{8,0},{10,2},{12,4},{14,6},{1,9},{3,11}... | collective-permute-start | bytes 319496 | tf_op jit(solution)/shard_map/ppermute | solution.py:22
  181.7 26.8 %copy-start.2 = (bf16[32,32,256]{2,1,0:T(8,128)(2,1)S(1)}, bf16[32,32,256]{2,1,0:T(8,128)(2,1)}, u32[]{:S(2)}) copy-start(bf16[32,32,256]{2,1,0:T(8,128)(2,1)} %pad_maximum_fusion.5) | copy-start | bytes 1572868
  210.3 0.7 slice-start
  210.3 1.0 copy-start.25
  212.9 3.8 %collective-permute-start.10 = (bf16[2048,128]{1,0:T(8,128)(2,1)S(1)}, bf16[2048,128]{1,0:T(8,128)(2,1)S(1)}, u32[]{:S(2)}, u32[]{:S(2)}) collective-permute-start(bf16[2048,128]{1,0:T(8,128)(2,1)S(1)} %bitcast.118), channel_id=1, source_target_pairs={{0,1},{1,0},{2,3},{3,2},{4,5},{5,4},{6,7},{7,6},{8,9},{9,8},{10,11... | collective-permute-start | bytes 1572872 | tf_op jit(solution)/shard_map/ppermute | solution.py:48
  217.7 41.3 %all-to-all-start.3 = ((bf16[16,128,128]{2,1,0:T(8,128)(2,1)}), bf16[16,128,128]{2,1,0:T(8,128)(2,1)S(1)}, u32[]{:S(2)}, u32[]{:S(2)}) async-start(bf16[16,128,128]{2,1,0:T(8,128)(2,1)} %fusion.6), calls=%async_computation.3 | async-start | bytes 1048576 | tf_op jit(solution)/shard_map/all_to_all | solution.py:17

commit v2 on v0

--- a/solution.py
+++ b/solution.py
@@ -7,6 +7,8 @@
 
 CAPACITY = 24
 TP = ("tp_0", "tp_1")
+FS = ("fs_0", "fs_1")
+NEAR = 4
 
 
 norm_eps = 1e-05
@@ -73,7 +75,8 @@
     shared_up,
     shared_down,
 ):
-    shards = lax.axis_size("fs")
+    shards = lax.axis_size(FS)
+    far, near = lax.axis_size("fs_0"), lax.axis_size("fs_1")
     chips = lax.axis_size("tp_0")
     core = lax.axis_index("tp_1")
     experts_all, unit_rows, slice_width = gate_weight.shape
@@ -93,7 +96,8 @@
 
     route_weight = route_scores / jnp.sum(route_scores, axis=1, keepdims=True) * routed_scale
     sent = jnp.concatenate([normed, expert_ids.T.astype(bf16), route_weight.T.astype(bf16)])
-    blocks = copy_for_each(sent, "fs")
+    blocks = copy_for_each(sent, "fs_0")
+    blocks = copy_for_each(blocks, "fs_1")
 
     gain = norm_gain[None, None, :]
     both_new = jnp.concatenate(
@@ -105,7 +109,7 @@
     three_new = jnp.concatenate([both_new, down_new], axis=1)
     three_sent = three_new.reshape(shards, experts_here, 3 * unit_rows, slice_width)
     three_sent = with_shared(three_sent, jnp.concatenate([both_shared, down_shared]))
-    served = exchange(tie(three_sent, blocks), "fs")
+    served = exchange(tie(three_sent, blocks), FS)
 
     def over_both(local, shared_local):
         rows = local.shape[1]
@@ -121,6 +125,7 @@
     down_pair, down_shared_pair = over_both(down_new, down_shared)
 
     blocks = tie(blocks, (both_pair, both_shared_pair, down_pair, down_shared_pair))
+    blocks = blocks.transpose(1, 0, 2, 3).reshape(shards, *sent.shape)
     own_tokens = blocks[:, :tok_rows]
     partner_tokens = swap_cores(own_tokens)
     all_tokens = jnp.concatenate([own_tokens, partner_tokens], axis=2)
@@ -191,7 +196,9 @@
         total[:, :, slice_width:].astype(bf16).reshape(-1, slice_width)
     ).reshape(shards, tok_rows, slice_width).astype(float32)
     served = tie(served, hidden)
-    partials = exchange(tie(total.astype(bf16), served), "fs")
+    total = total.astype(bf16).reshape(far, near, tok_rows, slice_width).transpose(1, 0, 2, 3)
+    partials = exchange(tie(total, served), "fs_1")
+    partials = exchange(jnp.sum(partials.astype(float32), axis=0).astype(bf16), "fs_0")
     layer_out = jnp.sum(partials.astype(float32), axis=0).astype(bf16)
 
     served = served.reshape(shards, experts_here + 1, 3, unit_rows, slice_width)
@@ -211,33 +218,33 @@
 
 
 def solution(mesh):
+    groups, shards, width = (mesh.shape[name] for name in ("grp", "fs", "tp"))
     split = Mesh(
-        mesh.devices.reshape(mesh.shape["grp"], mesh.shape["fs"], mesh.shape["tp"] // 2, 2),
-        ("grp", "fs", "tp_0", "tp_1"),
+        mesh.devices.reshape(groups, shards // NEAR, NEAR, width // 2, 2), ("grp", *FS, *TP)
     )
     return jax.shard_map(
         layer,
         mesh=split,
         in_specs=(
-            P(("grp", "fs"), TP),
+            P(("grp", *FS), TP),
             P(TP),
-            P(("grp", "fs"), None),
-            P(("grp", "fs"), None),
-            P(None, "fs", TP),
-            P(None, "fs", TP),
-            P(None, "fs", TP),
-            P("fs", TP),
-            P("fs", TP),
-            P("fs", TP),
+            P(("grp", *FS), None),
+            P(("grp", *FS), None),
+            P(None, FS, TP),
+            P(None, FS, TP),
+            P(None, FS, TP),
+            P(FS, TP),
+            P(FS, TP),
+            P(FS, TP),
         ),
         out_specs=(
-            P(("grp", "fs"), None, TP),
-            P(("grp", "fs"), None, TP),
-            P(("grp", "fs"), None, TP),
+            P(("grp", *FS), None, TP),
+            P(("grp", *FS), None, TP),
+            P(("grp", *FS), None, TP),
             P("grp", TP),
             P("grp", TP),
             P("grp", TP),
-            P(("grp", "fs"), TP),
+            P(("grp", *FS), TP),
         ),
         check_vma=False,
     )

time: 249 us -> 250 us (level)
  blocking collectives: 26.7 us -> 97.7 us
  starting transfers between devices: 105 us -> 66.1 us
  waiting for transfers between devices: 73.4 us -> 43.1 us
    all_to_all x0 -> x2, blocking collectives: none -> 71 us  [exchange(): return lax.all_to_all(array, axis, 0, 0, tiled=True)]
    all_to_all x4, starting transfers between devices: 71 us -> 32.3 us  [exchange(): return lax.all_to_all(array, axis, 0, 0, tiled=True)]
    all_to_all x4, waiting for transfers between devices: 57.2 us -> 26.9 us  [exchange(): return lax.all_to_all(array, axis, 0, 0, tiled=True)]
  transfers between devices with their start and end apart: 15 -> 15, of which waited for: 9 -> 9; matrix products, arithmetic and copies ran while one was open for 15% -> 14% of each run, Pallas kernels for 0% -> 0%
where the time goes in v2:
time: 250 us; the launch traced here: 249 us
  blocking collectives  97.7 us (39%)
  starting transfers between devices  66.1 us (26%)
  waiting for transfers between devices  43.1 us (17%)
  other arithmetic  21.7 us (9%)
  local copies, waits for them, and re-layouts  10.8 us (4%)
  matrix products  8.13 us (3%)
    all_to_all x2, blocking collectives, exchange(): return lax.all_to_all(array, axis, 0, 0, tiled=True)  71 us
    all_to_all x4, starting transfers between devices, exchange(): return lax.all_to_all(array, axis, 0, 0, tiled=True)  32.3 us
    all_to_all x4, waiting for transfers between devices, exchange(): return lax.all_to_all(array, axis, 0, 0, tiled=True)  26.9 us
    all_gather x1, blocking collectives, layer(): hidden = lax.all_gather(part.reshape(-1, lanes), 'tp_0')  26.7 us
    ppermute x7, starting transfers between devices, rotated(): lax.ppermute(array, axis, [(i, (i + by) % size) for i in range(size)])  25 us
    ppermute x7, waiting for transfers between devices, rotated(): lax.ppermute(array, axis, [(i, (i + by) % size) for i in range(size)])  13.4 us
    ppermute x4, starting transfers between devices, swap_cores(): return lax.ppermute(array, 'tp_1', [(0, 1), (1, 0)])  8.77 us
  transfers between devices with their start and end apart: 15, of which 9 were waited for; matrix products, arithmetic and copies ran while one was open for 14% of the time, Pallas kernels for 0%

profile of v2, /device:TPU:80, one launch (start us, length us, event | category | flops | bytes accessed | tf_op | source)
XLA Modules:
  0.0 249.1 jit_solution(11122301038173650597)
XLA Ops:
  0.6 1.0 convert_reduce_fusion
  2.2 7.8 %all-to-all-start = ((f32[16,2,128]{2,1,0:T(2,128)}), f32[16,2,128]{2,1,0:T(2,128)S(1)}, u32[]{:S(2)}, u32[]{:S(2)}) async-start(f32[16,2,128]{2,1,0:T(2,128)} %broadcast_in_dim.53), calls=%async_computation | async-start | bytes 32768 | tf_op jit(solution)/shard_map/all_to_all | solution.py:19
  12.1 5.3 %all-to-all-done = f32[16,2,128]{2,1,0:T(2,128)S(1)} async-done(((f32[16,2,128]{2,1,0:T(2,128)}), f32[16,2,128]{2,1,0:T(2,128)S(1)}, u32[]{:S(2)}, u32[]{:S(2)}) %all-to-all-start) | async-done | bytes 16416 | tf_op jit(solution)/shard_map/all_to_all | solution.py:19
  17.5 0.9 fusion.36
  18.4 51.7 %all_to_all.30 = bf16[4,144,128]{2,1,0:T(8,128)(2,1)S(1)} all-to-all(bf16[4,144,128]{2,1,0:T(8,128)(2,1)S(1)} %broadcast_in_dim.54), channel_id=1, replica_groups=mesh['grp'=2,'fs_0'=4,'fs_1'=4,'tp_0'=8,'tp_1'=2] {'fs_0'}, dimensions={0} | all-to-all | bytes 294912 | tf_op jit(solution)/shard_map/all_to_all | solution.py:19
  70.1 0.9 broadcast_in_dim.55
  71.0 9.4 %all-to-all-start.2 = ((bf16[4,4,144,128]{3,2,1,0:T(8,128)(2,1)}), bf16[4,4,144,128]{3,2,1,0:T(8,128)(2,1)}, u32[]{:S(2)}, u32[]{:S(2)}) async-start(bf16[4,4,144,128]{3,2,1,0:T(8,128)(2,1)} %broadcast_in_dim.55), calls=%async_computation.2 | async-start | bytes 1179648 | tf_op jit(solution)/shard_map/all_to_all | solution.py:19
  81.1 1.8 multiply_convert_fusion.1
  83.0 1.5 pad_maximum_fusion
  84.5 11.0 %all-to-all-done.2 = bf16[4,4,144,128]{3,2,1,0:T(8,128)(2,1)} async-done(((bf16[4,4,144,128]{3,2,1,0:T(8,128)(2,1)}), bf16[4,4,144,128]{3,2,1,0:T(8,128)(2,1)}, u32[]{:S(2)}, u32[]{:S(2)}) %all-to-all-start.2) | async-done | bytes 589856 | tf_op jit(solution)/shard_map/all_to_all | solution.py:19
  95.5 5.4 %all-to-all-start.3 = ((bf16[16,5,96,128]{3,2,1,0:T(8,128)(2,1)}), bf16[16,5,96,128]{3,2,1,0:T(8,128)(2,1)S(1)}, u32[]{:S(2)}, u32[]{:S(2)}) async-start(bf16[16,5,96,128]{3,2,1,0:T(8,128)(2,1)} %pad_maximum_fusion), calls=%async_computation.3 | async-start | bytes 3932160 | tf_op jit(solution)/shard_map/all_to_all | solution.py:19
  101.0 1.0 fusion.11
  101.9 0.8 maximum_maximum_fusion
  102.8 1.9 collective-permute-start
  104.8 2.6 %collective-permute-start.1 = (bf16[1056,128]{1,0:T(8,128)(2,1)S(1)}, bf16[1056,128]{1,0:T(8,128)(2,1)S(1)}, u32[]{:S(2)}, u32[]{:S(2)}) collective-permute-start(bf16[1056,128]{1,0:T(8,128)(2,1)S(1)} %bitcast.129), channel_id=1, source_target_pairs={{0,1},{1,0},{2,3},{3,2},{4,5},{5,4},{6,7},{7,6},{8,9},{9,8},{10,11... | collective-permute-start | bytes 811016 | tf_op jit(solution)/shard_map/ppermute | solution.py:44
  107.6 0.9 collective-permute-done.1
  108.6 0.9 pad_maximum_fusion.5
  109.5 1.1 slice.114
  111.4 1.1 copy.52
  112.6 2.3 collective-permute-start.2
  116.4 1.0 bitcast_compare_fusion
  117.5 1.8 convolution_convert_fusion.1
  120.4 2.3 convolution_convert_fusion.2
  122.7 1.1 fusion.32
  123.8 2.6 %collective-permute-start.3 = (bf16[832,128]{1,0:T(8,128)(2,1)}, bf16[832,128]{1,0:T(8,128)(2,1)}, u32[]{:S(2)}, u32[]{:S(2)}) collective-permute-start(bf16[832,128]{1,0:T(8,128)(2,1)} %get-tuple-element.23), channel_id=1, source_target_pairs={{0,8},{2,10},{4,12},{6,14},{8,0},{10,2},{12,4},{14,6},{1,9},{3,11}... | collective-permute-start | bytes 638984 | tf_op jit(solution)/shard_map/ppermute | solution.py:24
  126.4 5.1 %collective-permute-start.4 = (bf16[832,128]{1,0:T(8,128)(2,1)}, bf16[832,128]{1,0:T(8,128)(2,1)}, u32[]{:S(2)}, u32[]{:S(2)}) collective-permute-start(bf16[832,128]{1,0:T(8,128)(2,1)} %get-tuple-element.24), channel_id=1, source_target_pairs={{0,6},{2,8},{4,10},{6,12},{8,14},{10,0},{12,2},{14,4},{1,7},{3,9},... | collective-permute-start | bytes 638984 | tf_op jit(solution)/shard_map/ppermute | solution.py:24
  131.5 3.8 %collective-permute-start.5 = (bf16[832,128]{1,0:T(8,128)(2,1)}, bf16[832,128]{1,0:T(8,128)(2,1)}, u32[]{:S(2)}, u32[]{:S(2)}) collective-permute-start(bf16[832,128]{1,0:T(8,128)(2,1)} %get-tuple-element.25), channel_id=1, source_target_pairs={{0,10},{2,12},{4,14},{6,0},{8,2},{10,4},{12,6},{14,8},{1,11},{3,13... | collective-permute-start | bytes 638984 | tf_op jit(solution)/shard_map/ppermute | solution.py:24
  135.3 4.2 %collective-permute-start.6 = (bf16[832,128]{1,0:T(8,128)(2,1)}, bf16[832,128]{1,0:T(8,128)(2,1)}, u32[]{:S(2)}, u32[]{:S(2)}) collective-permute-start(bf16[832,128]{1,0:T(8,128)(2,1)} %get-tuple-element.26), channel_id=1, source_target_pairs={{0,4},{2,6},{4,8},{6,10},{8,12},{10,14},{12,0},{14,2},{1,5},{3,7},... | collective-permute-start | bytes 638984 | tf_op jit(solution)/shard_map/ppermute | solution.py:24
  139.5 3.8 %collective-permute-start.7 = (bf16[832,128]{1,0:T(8,128)(2,1)}, bf16[832,128]{1,0:T(8,128)(2,1)}, u32[]{:S(2)}, u32[]{:S(2)}) collective-permute-start(bf16[832,128]{1,0:T(8,128)(2,1)} %get-tuple-element.27), channel_id=1, source_target_pairs={{0,12},{2,14},{4,0},{6,2},{8,4},{10,6},{12,8},{14,10},{1,13},{3,15... | collective-permute-start | bytes 638984 | tf_op jit(solution)/shard_map/ppermute | solution.py:24
  143.3 1.4 fusion.33
  145.4 2.7 %collective-permute-start.8 = (bf16[832,128]{1,0:T(8,128)(2,1)}, bf16[832,128]{1,0:T(8,128)(2,1)}, u32[]{:S(2)}, u32[]{:S(2)}) collective-permute-start(bf16[832,128]{1,0:T(8,128)(2,1)} %get-tuple-element.28), channel_id=1, source_target_pairs={{0,2},{2,4},{4,6},{6,8},{8,10},{10,12},{12,14},{14,0},{1,3},{3,5},... | collective-permute-start | bytes 638984 | tf_op jit(solution)/shard_map/ppermute | solution.py:24
  148.1 7.7 %collective-permute-done.4 = bf16[832,128]{1,0:T(8,128)(2,1)} collective-permute-done((bf16[832,128]{1,0:T(8,128)(2,1)}, bf16[832,128]{1,0:T(8,128)(2,1)}, u32[]{:S(2)}, u32[]{:S(2)}) %collective-permute-start.4) | collective-permute-done | bytes 213024 | tf_op jit(solution)/shard_map/ppermute | solution.py:24
  155.9 2.8 %collective-permute-start.9 = (bf16[832,128]{1,0:T(8,128)(2,1)}, bf16[832,128]{1,0:T(8,128)(2,1)}, u32[]{:S(2)}, u32[]{:S(2)}) collective-permute-start(bf16[832,128]{1,0:T(8,128)(2,1)} %fusion.33), channel_id=1, source_target_pairs={{0,14},{2,0},{4,2},{6,4},{8,6},{10,8},{12,10},{14,12},{1,15},{3,1}... | collective-permute-start | bytes 638984 | tf_op jit(solution)/shard_map/ppermute | solution.py:24
  159.2 1.2 fusion.1
  160.5 1.9 fusion
  163.2 4.2 %collective-permute-done.8 = bf16[832,128]{1,0:T(8,128)(2,1)} collective-permute-done((bf16[832,128]{1,0:T(8,128)(2,1)}, bf16[832,128]{1,0:T(8,128)(2,1)}, u32[]{:S(2)}, u32[]{:S(2)}) %collective-permute-start.8) | collective-permute-done | bytes 213024 | tf_op jit(solution)/shard_map/ppermute | solution.py:24
  167.4 1.7 fusion.17
  169.1 26.7 %all_gather.3 = bf16[8,416,128]{2,1,0:T(8,128)(2,1)S(1)} all-gather(bf16[1,416,128]{2,1,0:T(8,128)(2,1)S(1)} %bitcast.128), channel_id=1, replica_groups=mesh['grp'=2,'fs_0'=4,'fs_1'=4,'tp_0'=8,'tp_1'=2] {'tp_0'}, dimensions={0}, use_global_device_ids=true | all-gather | bytes 958464 | tf_op jit(solution)/shard_map/all_gather | solution.py:178
  195.9 1.8 convolution_convert_fusion
  198.8 1.4 fusion.2
  200.3 2.0 collective-permute-start.10
  202.3 1.9 collective-permute-done.10
  204.4 19.3 %all_to_all.31 = bf16[4,4,128,128]{3,2,1,0:T(8,128)(2,1)S(1)} all-to-all(bf16[4,4,128,128]{3,2,1,0:T(8,128)(2,1)S(1)} %bitcast.118), channel_id=1, replica_groups=mesh['grp'=2,'fs_0'=4,'fs_1'=4,'tp_0'=8,'tp_1'=2] {'fs_1'}, dimensions={0} | all-to-all | bytes 1048576 | tf_op jit(solution)/shard_map/all_to_all | solution.py:19
  224.5 9.8 %all-to-all-start.5 = ((bf16[4,128,128]{2,1,0:T(8,128)(2,1)}), bf16[4,128,128]{2,1,0:T(8,128)(2,1)S(1)}, u32[]{:S(2)}, u32[]{:S(2)}) async-start(bf16[4,128,128]{2,1,0:T(8,128)(2,1)} %reduce_sum.74), calls=%async_computation.5 | async-start | bytes 262144 | tf_op jit(solution)/shard_map/all_to_all | solution.py:19
  234.7 0.8 copy.54
  235.6 0.8 copy.55
  236.4 0.8 copy.56
  238.0 10.5 %all-to-all-done.5 = bf16[4,128,128]{2,1,0:T(8,128)(2,1)S(1)} async-done(((bf16[4,128,128]{2,1,0:T(8,128)(2,1)}), bf16[4,128,128]{2,1,0:T(8,128)(2,1)S(1)}, u32[]{:S(2)}, u32[]{:S(2)}) %all-to-all-start.5) | async-done | bytes 131104 | tf_op jit(solution)/shard_map/all_to_all | solution.py:19
  (99 shorter events, 13.3 us)
Async XLA Ops:
  0.6 79.7 %copy-start.5 = (f32[64,32,128]{2,1,0:T(8,128)S(1)}, f32[64,32,128]{2,1,0:T(8,128)}, u32[]{:S(2)}) copy-start(f32[64,32,128]{2,1,0:T(8,128)} %param.16) | copy-start | bytes 3145732
  1.6 78.8 %copy-start.13 = (f32[32,128]{1,0:T(8,128)S(1)}, f32[32,128]{1,0:T(8,128)}, u32[]{:S(2)}) copy-start(f32[32,128]{1,0:T(8,128)} %param.19) | copy-start | bytes 49156
  2.2 78.2 %copy-start.17 = (f32[32,128]{1,0:T(8,128)S(1)}, f32[32,128]{1,0:T(8,128)}, u32[]{:S(2)}) copy-start(f32[32,128]{1,0:T(8,128)} %param.17) | copy-start | bytes 49156
  2.2 78.2 %copy-start.18 = (f32[32,128]{1,0:T(8,128)S(1)}, f32[32,128]{1,0:T(8,128)}, u32[]{:S(2)}) copy-start(f32[32,128]{1,0:T(8,128)} %param.18) | copy-start | bytes 49156
  2.2 78.2 %copy-start.21 = (f32[128]{0:T(128)S(1)}, f32[128]{0:T(128)}, u32[]{:S(2)}) copy-start(f32[128]{0:T(128)} %param.11) | copy-start | bytes 1540
  2.2 15.2 %all-to-all-start = ((f32[16,2,128]{2,1,0:T(2,128)}), f32[16,2,128]{2,1,0:T(2,128)S(1)}, u32[]{:S(2)}, u32[]{:S(2)}) async-start(f32[16,2,128]{2,1,0:T(2,128)} %broadcast_in_dim.53), calls=%async_computation | async-start | bytes 32768 | tf_op jit(solution)/shard_map/all_to_all | solution.py:19
  71.0 24.6 %all-to-all-start.2 = ((bf16[4,4,144,128]{3,2,1,0:T(8,128)(2,1)}), bf16[4,4,144,128]{3,2,1,0:T(8,128)(2,1)}, u32[]{:S(2)}, u32[]{:S(2)}) async-start(bf16[4,4,144,128]{3,2,1,0:T(8,128)(2,1)} %broadcast_in_dim.55), calls=%async_computation.2 | async-start | bytes 1179648 | tf_op jit(solution)/shard_map/all_to_all | solution.py:19
  80.5 0.6 copy-start.10
  80.5 21.4 %copy-start.8 = (bf16[32,128]{1,0:T(8,128)(2,1)}, bf16[32,128]{1,0:T(8,128)(2,1)S(1)}, u32[]{:S(2)}) copy-start(bf16[32,128]{1,0:T(8,128)(2,1)S(1)} %get-tuple-element.37) | copy-start | bytes 24580
  95.5 108.8 %all-to-all-start.3 = ((bf16[16,5,96,128]{3,2,1,0:T(8,128)(2,1)}), bf16[16,5,96,128]{3,2,1,0:T(8,128)(2,1)S(1)}, u32[]{:S(2)}, u32[]{:S(2)}) async-start(bf16[16,5,96,128]{3,2,1,0:T(8,128)(2,1)} %pad_maximum_fusion), calls=%async_computation.3 | async-start | bytes 3932160 | tf_op jit(solution)/shard_map/all_to_all | solution.py:19
  100.9 1.0 copy-start.11
  100.9 3.8 %copy-start.14 = (f32[32,128]{1,0:T(8,128)S(1)}, f32[32,128]{1,0:T(8,128)}, u32[]{:S(2)}) copy-start(f32[32,128]{1,0:T(8,128)} %param.19) | copy-start | bytes 49156
  102.8 6.7 %collective-permute-start = (bf16[2112,128]{1,0:T(8,128)(2,1)}, bf16[2112,128]{1,0:T(8,128)(2,1)}, u32[]{:S(2)}, u32[]{:S(2)}) collective-permute-start(bf16[2112,128]{1,0:T(8,128)(2,1)} %bitcast.9), channel_id=1, source_target_pairs={{0,1},{1,0},{2,3},{3,2},{4,5},{5,4},{6,7},{7,6},{8,9},{9,8},{10,11... | collective-permute-start | bytes 1622024 | tf_op jit(solution)/shard_map/ppermute | solution.py:44
  104.7 6.5 %copy-start.1 = (bf16[32,64,128]{2,1,0:T(8,128)(2,1)S(1)}, bf16[32,64,128]{2,1,0:T(8,128)(2,1)}, u32[]{:S(2)}) copy-start(bf16[32,64,128]{2,1,0:T(8,128)(2,1)} %get-tuple-element.29) | copy-start | bytes 1572868
  104.8 3.7 %collective-permute-start.1 = (bf16[1056,128]{1,0:T(8,128)(2,1)S(1)}, bf16[1056,128]{1,0:T(8,128)(2,1)S(1)}, u32[]{:S(2)}, u32[]{:S(2)}) collective-permute-start(bf16[1056,128]{1,0:T(8,128)(2,1)S(1)} %bitcast.129), channel_id=1, source_target_pairs={{0,1},{1,0},{2,3},{3,2},{4,5},{5,4},{6,7},{7,6},{8,9},{9,8},{10,11... | collective-permute-start | bytes 811016 | tf_op jit(solution)/shard_map/ppermute | solution.py:44
  107.6 8.8 %copy-start.15 = (s32[768]{0:T(1024)}, s32[768]{0:T(1024)S(1)}, u32[]{:S(2)}) copy-start(s32[768]{0:T(1024)S(1)} %eq.60) | copy-start | bytes 9220
  107.6 7.9 %copy-start.19 = (s32[32]{0:T(128)}, s32[32]{0:T(128)S(1)}, u32[]{:S(2)}) copy-start(s32[32]{0:T(128)S(1)} %iota_add_fusion) | copy-start | bytes 388
  108.6 2.9 %copy-start.7 = (bf16[1056,128]{1,0:T(8,128)(2,1)}, bf16[1056,128]{1,0:T(8,128)(2,1)S(1)}, u32[]{:S(2)}) copy-start(bf16[1056,128]{1,0:T(8,128)(2,1)S(1)} %collective-permute-done.1) | copy-start | bytes 811012
  112.6 4.9 %collective-permute-start.2 = (bf16[16,128,128]{2,1,0:T(8,128)(2,1)S(1)}, bf16[16,128,128]{2,1,0:T(8,128)(2,1)S(1)}, u32[]{:S(2)}, u32[]{:S(2)}) collective-permute-start(bf16[16,128,128]{2,1,0:T(8,128)(2,1)S(1)} %slice.119), channel_id=1, source_target_pairs={{0,1},{1,0},{2,3},{3,2},{4,5},{5,4},{6,7},{7,6},{8,9},{9,8},{10,11... | collective-permute-start | bytes 1572872 | tf_op jit(solution)/shard_map/ppermute | solution.py:44
  115.6 0.6 copy-start.6
  116.4 1.1 copy-start
  119.2 0.8 copy-start.9
  119.3 0.8 copy-start.12
  120.3 2.3 copy-start.3
  122.7 36.6 %copy-start.20 = (s32[32]{0:T(128)S(1)}, s32[32]{0:T(128)}, u32[]{:S(2)}) copy-start(s32[32]{0:T(128)} %copy-done.19) | copy-start | bytes 388
  122.7 37.8 %copy-start.16 = (s32[768]{0:T(1024)S(1)}, s32[768]{0:T(1024)}, u32[]{:S(2)}) copy-start(s32[768]{0:T(1024)} %copy-done.15) | copy-start | bytes 9220
  123.8 21.7 %collective-permute-start.3 = (bf16[832,128]{1,0:T(8,128)(2,1)}, bf16[832,128]{1,0:T(8,128)(2,1)}, u32[]{:S(2)}, u32[]{:S(2)}) collective-permute-start(bf16[832,128]{1,0:T(8,128)(2,1)} %get-tuple-element.23), channel_id=1, source_target_pairs={{0,8},{2,10},{4,12},{6,14},{8,0},{10,2},{12,4},{14,6},{1,9},{3,11}... | collective-permute-start | bytes 638984 | tf_op jit(solution)/shard_map/ppermute | solution.py:24
  126.4 29.5 %collective-permute-start.4 = (bf16[832,128]{1,0:T(8,128)(2,1)}, bf16[832,128]{1,0:T(8,128)(2,1)}, u32[]{:S(2)}, u32[]{:S(2)}) collective-permute-start(bf16[832,128]{1,0:T(8,128)(2,1)} %get-tuple-element.24), channel_id=1, source_target_pairs={{0,6},{2,8},{4,10},{6,12},{8,14},{10,0},{12,2},{14,4},{1,7},{3,9},... | collective-permute-start | bytes 638984 | tf_op jit(solution)/shard_map/ppermute | solution.py:24
  131.5 30.9 %collective-permute-start.5 = (bf16[832,128]{1,0:T(8,128)(2,1)}, bf16[832,128]{1,0:T(8,128)(2,1)}, u32[]{:S(2)}, u32[]{:S(2)}) collective-permute-start(bf16[832,128]{1,0:T(8,128)(2,1)} %get-tuple-element.25), channel_id=1, source_target_pairs={{0,10},{2,12},{4,14},{6,0},{8,2},{10,4},{12,6},{14,8},{1,11},{3,13... | collective-permute-start | bytes 638984 | tf_op jit(solution)/shard_map/ppermute | solution.py:24
  135.3 27.1 %collective-permute-start.6 = (bf16[832,128]{1,0:T(8,128)(2,1)}, bf16[832,128]{1,0:T(8,128)(2,1)}, u32[]{:S(2)}, u32[]{:S(2)}) collective-permute-start(bf16[832,128]{1,0:T(8,128)(2,1)} %get-tuple-element.26), channel_id=1, source_target_pairs={{0,4},{2,6},{4,8},{6,10},{8,12},{10,14},{12,0},{14,2},{1,5},{3,7},... | collective-permute-start | bytes 638984 | tf_op jit(solution)/shard_map/ppermute | solution.py:24
  139.5 23.7 %collective-permute-start.7 = (bf16[832,128]{1,0:T(8,128)(2,1)}, bf16[832,128]{1,0:T(8,128)(2,1)}, u32[]{:S(2)}, u32[]{:S(2)}) collective-permute-start(bf16[832,128]{1,0:T(8,128)(2,1)} %get-tuple-element.27), channel_id=1, source_target_pairs={{0,12},{2,14},{4,0},{6,2},{8,4},{10,6},{12,8},{14,10},{1,13},{3,15... | collective-permute-start | bytes 638984 | tf_op jit(solution)/shard_map/ppermute | solution.py:24
  145.4 21.9 %collective-permute-start.8 = (bf16[832,128]{1,0:T(8,128)(2,1)}, bf16[832,128]{1,0:T(8,128)(2,1)}, u32[]{:S(2)}, u32[]{:S(2)}) collective-permute-start(bf16[832,128]{1,0:T(8,128)(2,1)} %get-tuple-element.28), channel_id=1, source_target_pairs={{0,2},{2,4},{4,6},{6,8},{8,10},{10,12},{12,14},{14,0},{1,3},{3,5},... | collective-permute-start | bytes 638984 | tf_op jit(solution)/shard_map/ppermute | solution.py:24
  155.9 11.5 %collective-permute-start.9 = (bf16[832,128]{1,0:T(8,128)(2,1)}, bf16[832,128]{1,0:T(8,128)(2,1)}, u32[]{:S(2)}, u32[]{:S(2)}) collective-permute-start(bf16[832,128]{1,0:T(8,128)(2,1)} %fusion.33), channel_id=1, source_target_pairs={{0,14},{2,0},{4,2},{6,4},{8,6},{10,8},{12,10},{14,12},{1,15},{3,1}... | collective-permute-start | bytes 638984 | tf_op jit(solution)/shard_map/ppermute | solution.py:24
  159.2 8.2 %copy-start.4 = (bf16[8,64,128]{2,1,0:T(8,128)(2,1)S(1)}, bf16[8,64,128]{2,1,0:T(8,128)(2,1)}, u32[]{:S(2)}) copy-start(bf16[8,64,128]{2,1,0:T(8,128)(2,1)} %copy-done.3) | copy-start | bytes 393220
  169.1 26.9 %copy-start.2 = (bf16[32,32,256]{2,1,0:T(8,128)(2,1)S(1)}, bf16[32,32,256]{2,1,0:T(8,128)(2,1)}, u32[]{:S(2)}) copy-start(bf16[32,32,256]{2,1,0:T(8,128)(2,1)} %pad_maximum_fusion.5) | copy-start | bytes 1572868
  197.8 0.7 slice-start
  197.8 1.0 copy-start.22
  200.3 3.8 %collective-permute-start.10 = (bf16[2048,128]{1,0:T(8,128)(2,1)S(1)}, bf16[2048,128]{1,0:T(8,128)(2,1)S(1)}, u32[]{:S(2)}, u32[]{:S(2)}) collective-permute-start(bf16[2048,128]{1,0:T(8,128)(2,1)S(1)} %bitcast.126), channel_id=1, source_target_pairs={{0,1},{1,0},{2,3},{3,2},{4,5},{5,4},{6,7},{7,6},{8,9},{9,8},{10,11... | collective-permute-start | bytes 1572872 | tf_op jit(solution)/shard_map/ppermute | solution.py:44
  224.5 24.0 %all-to-all-start.5 = ((bf16[4,128,128]{2,1,0:T(8,128)(2,1)}), bf16[4,128,128]{2,1,0:T(8,128)(2,1)S(1)}, u32[]{:S(2)}, u32[]{:S(2)}) async-start(bf16[4,128,128]{2,1,0:T(8,128)(2,1)} %reduce_sum.74), calls=%async_computation.5 | async-start | bytes 262144 | tf_op jit(solution)/shard_map/all_to_all | solution.py:19

commit v3 on v0

--- a/solution.py
+++ b/solution.py
@@ -84,8 +84,9 @@
     float32 = jnp.float32
 
     tok_float = tokens.astype(float32)
-    sums = jnp.stack([jnp.sum(tok_float, axis=1), jnp.sum(tok_float * tok_float, axis=1)])
-    row_sum, row_squares = jnp.sum(copy_for_each(sums, TP), axis=0)
+    sums = jnp.concatenate([jnp.sum(tok_float, axis=1), jnp.sum(tok_float * tok_float, axis=1)])
+    sums = jnp.sum(copy_for_each(sums, TP), axis=0)
+    row_sum, row_squares = sums[:tok_rows], sums[tok_rows:]
     full_width = slice_width * lax.axis_size(TP)
     row_mean = row_sum / full_width
     row_var = row_squares / full_width - row_mean * row_mean

time: 249 us -> 249 us (level)
  no operation moved by 1% of the time
where the time goes in v3:
time: 249 us; the launch traced here: 248 us
  starting transfers between devices  105 us (42%)
  waiting for transfers between devices  73.4 us (29%)
  blocking collectives  26.7 us (11%)
  other arithmetic  22.4 us (9%)
  local copies, waits for them, and re-layouts  11.2 us (4%)
  matrix products  8.15 us (3%)
    all_to_all x4, starting transfers between devices, exchange(): return lax.all_to_all(array, axis, 0, 0, tiled=True)  71 us
    all_to_all x4, waiting for transfers between devices, exchange(): return lax.all_to_all(array, axis, 0, 0, tiled=True)  57.2 us
    all_gather x1, blocking collectives, layer(): hidden = lax.all_gather(part.reshape(-1, lanes), 'tp_0')  26.7 us
    ppermute x7, starting transfers between devices, rotated(): lax.ppermute(array, axis, [(i, (i + by) % size) for i in range(size)])  25 us
    ppermute x7, waiting for transfers between devices, rotated(): lax.ppermute(array, axis, [(i, (i + by) % size) for i in range(size)])  13.4 us
    ppermute x4, starting transfers between devices, swap_cores(): return lax.ppermute(array, 'tp_1', [(0, 1), (1, 0)])  8.77 us
  transfers between devices with their start and end apart: 15, of which 9 were waited for; matrix products, arithmetic and copies ran while one was open for 15% of the time, Pallas kernels for 0%

profile of v3, /device:TPU:80, one launch (start us, length us, event | category | flops | bytes accessed | tf_op | source)
XLA Modules:
  0.0 248.0 jit_solution(17950167407898356992)
XLA Ops:
  0.7 0.9 convert_reduce_fusion
  2.3 7.6 %all-to-all-start = ((f32[16,1,256]{2,1,0:T(1,128)}), f32[16,1,256]{2,1,0:T(1,128)S(1)}, u32[]{:S(2)}, u32[]{:S(2)}) async-start(f32[16,1,256]{2,1,0:T(1,128)} %broadcast_in_dim.51), calls=%async_computation | async-start | bytes 32768 | tf_op jit(solution)/shard_map/all_to_all | solution.py:17
  12.0 5.3 %all-to-all-done = f32[16,1,256]{2,1,0:T(1,128)S(1)} async-done(((f32[16,1,256]{2,1,0:T(1,128)}), f32[16,1,256]{2,1,0:T(1,128)S(1)}, u32[]{:S(2)}, u32[]{:S(2)}) %all-to-all-start) | async-done | bytes 16416 | tf_op jit(solution)/shard_map/all_to_all | solution.py:17
  17.4 0.9 fusion.36
  18.3 0.9 broadcast_in_dim.52
  19.1 43.7 %all-to-all-start.1 = ((bf16[16,144,128]{2,1,0:T(8,128)(2,1)}), bf16[16,144,128]{2,1,0:T(8,128)(2,1)}, u32[]{:S(2)}, u32[]{:S(2)}) async-start(bf16[16,144,128]{2,1,0:T(8,128)(2,1)} %broadcast_in_dim.52), calls=%async_computation.1 | async-start | bytes 1179648 | tf_op jit(solution)/shard_map/all_to_all | solution.py:17
  64.1 1.5 multiply_convert_fusion.1
  65.7 1.5 pad_maximum_fusion
  67.2 26.5 %all-to-all-done.1 = bf16[16,144,128]{2,1,0:T(8,128)(2,1)} async-done(((bf16[16,144,128]{2,1,0:T(8,128)(2,1)}), bf16[16,144,128]{2,1,0:T(8,128)(2,1)}, u32[]{:S(2)}, u32[]{:S(2)}) %all-to-all-start.1) | async-done | bytes 589856 | tf_op jit(solution)/shard_map/all_to_all | solution.py:17
  93.7 7.7 %all-to-all-start.2 = ((bf16[16,5,96,128]{3,2,1,0:T(8,128)(2,1)}), bf16[16,5,96,128]{3,2,1,0:T(8,128)(2,1)S(1)}, u32[]{:S(2)}, u32[]{:S(2)}) async-start(bf16[16,5,96,128]{3,2,1,0:T(8,128)(2,1)} %pad_maximum_fusion), calls=%async_computation.2 | async-start | bytes 3932160 | tf_op jit(solution)/shard_map/all_to_all | solution.py:17
  101.5 1.0 fusion.11
  102.4 0.8 maximum_maximum_fusion
  103.3 1.9 collective-permute-start
  105.3 2.6 %collective-permute-start.1 = (bf16[1056,128]{1,0:T(8,128)(2,1)S(1)}, bf16[1056,128]{1,0:T(8,128)(2,1)S(1)}, u32[]{:S(2)}, u32[]{:S(2)}) collective-permute-start(bf16[1056,128]{1,0:T(8,128)(2,1)S(1)} %bitcast.107), channel_id=1, source_target_pairs={{0,1},{1,0},{2,3},{3,2},{4,5},{5,4},{6,7},{7,6},{8,9},{9,8},{10,11... | collective-permute-start | bytes 811016 | tf_op jit(solution)/shard_map/ppermute | solution.py:42
  108.1 0.9 collective-permute-done.1
  109.1 0.9 pad_maximum_fusion.5
  110.0 1.1 slice.122
  111.9 1.1 slice.105
  113.0 2.3 collective-permute-start.2
  115.3 1.4 slice_convert_fusion.1
  117.6 1.0 bitcast_compare_fusion
  118.7 1.8 convolution_convert_fusion.1
  121.6 2.3 convolution_convert_fusion.2
  123.9 1.1 fusion.32
  125.0 2.6 %collective-permute-start.3 = (bf16[832,128]{1,0:T(8,128)(2,1)}, bf16[832,128]{1,0:T(8,128)(2,1)}, u32[]{:S(2)}, u32[]{:S(2)}) collective-permute-start(bf16[832,128]{1,0:T(8,128)(2,1)} %get-tuple-element.23), channel_id=1, source_target_pairs={{0,8},{2,10},{4,12},{6,14},{8,0},{10,2},{12,4},{14,6},{1,9},{3,11}... | collective-permute-start | bytes 638984 | tf_op jit(solution)/shard_map/ppermute | solution.py:22
  127.6 5.1 %collective-permute-start.4 = (bf16[832,128]{1,0:T(8,128)(2,1)}, bf16[832,128]{1,0:T(8,128)(2,1)}, u32[]{:S(2)}, u32[]{:S(2)}) collective-permute-start(bf16[832,128]{1,0:T(8,128)(2,1)} %get-tuple-element.24), channel_id=1, source_target_pairs={{0,6},{2,8},{4,10},{6,12},{8,14},{10,0},{12,2},{14,4},{1,7},{3,9},... | collective-permute-start | bytes 638984 | tf_op jit(solution)/shard_map/ppermute | solution.py:22
  132.7 3.8 %collective-permute-start.5 = (bf16[832,128]{1,0:T(8,128)(2,1)}, bf16[832,128]{1,0:T(8,128)(2,1)}, u32[]{:S(2)}, u32[]{:S(2)}) collective-permute-start(bf16[832,128]{1,0:T(8,128)(2,1)} %get-tuple-element.25), channel_id=1, source_target_pairs={{0,10},{2,12},{4,14},{6,0},{8,2},{10,4},{12,6},{14,8},{1,11},{3,13... | collective-permute-start | bytes 638984 | tf_op jit(solution)/shard_map/ppermute | solution.py:22
  136.5 4.2 %collective-permute-start.6 = (bf16[832,128]{1,0:T(8,128)(2,1)}, bf16[832,128]{1,0:T(8,128)(2,1)}, u32[]{:S(2)}, u32[]{:S(2)}) collective-permute-start(bf16[832,128]{1,0:T(8,128)(2,1)} %get-tuple-element.26), channel_id=1, source_target_pairs={{0,4},{2,6},{4,8},{6,10},{8,12},{10,14},{12,0},{14,2},{1,5},{3,7},... | collective-permute-start | bytes 638984 | tf_op jit(solution)/shard_map/ppermute | solution.py:22
  140.8 3.8 %collective-permute-start.7 = (bf16[832,128]{1,0:T(8,128)(2,1)}, bf16[832,128]{1,0:T(8,128)(2,1)}, u32[]{:S(2)}, u32[]{:S(2)}) collective-permute-start(bf16[832,128]{1,0:T(8,128)(2,1)} %get-tuple-element.27), channel_id=1, source_target_pairs={{0,12},{2,14},{4,0},{6,2},{8,4},{10,6},{12,8},{14,10},{1,13},{3,15... | collective-permute-start | bytes 638984 | tf_op jit(solution)/shard_map/ppermute | solution.py:22
  144.6 1.4 fusion.33
  146.7 2.6 %collective-permute-start.8 = (bf16[832,128]{1,0:T(8,128)(2,1)}, bf16[832,128]{1,0:T(8,128)(2,1)}, u32[]{:S(2)}, u32[]{:S(2)}) collective-permute-start(bf16[832,128]{1,0:T(8,128)(2,1)} %get-tuple-element.28), channel_id=1, source_target_pairs={{0,2},{2,4},{4,6},{6,8},{8,10},{10,12},{12,14},{14,0},{1,3},{3,5},... | collective-permute-start | bytes 638984 | tf_op jit(solution)/shard_map/ppermute | solution.py:22
  149.3 7.8 %collective-permute-done.4 = bf16[832,128]{1,0:T(8,128)(2,1)} collective-permute-done((bf16[832,128]{1,0:T(8,128)(2,1)}, bf16[832,128]{1,0:T(8,128)(2,1)}, u32[]{:S(2)}, u32[]{:S(2)}) %collective-permute-start.4) | collective-permute-done | bytes 213024 | tf_op jit(solution)/shard_map/ppermute | solution.py:22
  157.1 2.8 %collective-permute-start.9 = (bf16[832,128]{1,0:T(8,128)(2,1)}, bf16[832,128]{1,0:T(8,128)(2,1)}, u32[]{:S(2)}, u32[]{:S(2)}) collective-permute-start(bf16[832,128]{1,0:T(8,128)(2,1)} %fusion.33), channel_id=1, source_target_pairs={{0,14},{2,0},{4,2},{6,4},{8,6},{10,8},{12,10},{14,12},{1,15},{3,1}... | collective-permute-start | bytes 638984 | tf_op jit(solution)/shard_map/ppermute | solution.py:22
  160.5 1.2 fusion.1
  161.7 1.9 fusion
  164.3 4.3 %collective-permute-done.8 = bf16[832,128]{1,0:T(8,128)(2,1)} collective-permute-done((bf16[832,128]{1,0:T(8,128)(2,1)}, bf16[832,128]{1,0:T(8,128)(2,1)}, u32[]{:S(2)}, u32[]{:S(2)}) %collective-permute-start.8) | collective-permute-done | bytes 213024 | tf_op jit(solution)/shard_map/ppermute | solution.py:22
  168.6 1.7 fusion.17
  170.4 26.7 %all_gather.3 = bf16[8,416,128]{2,1,0:T(8,128)(2,1)S(1)} all-gather(bf16[1,416,128]{2,1,0:T(8,128)(2,1)S(1)} %bitcast.106), channel_id=1, replica_groups=mesh['grp'=2,'fs'=16,'tp_0'=8,'tp_1'=2] {'tp_0'}, dimensions={0}, use_global_device_ids=true | all-gather | bytes 958464 | tf_op jit(solution)/shard_map/all_gather | solution.py:174
  197.1 1.8 convolution_convert_fusion
  200.0 1.4 fusion.2
  201.5 2.0 collective-permute-start.10
  203.5 1.9 collective-permute-done.10
  205.4 1.0 fusion.6
  206.3 12.0 %all-to-all-start.3 = ((bf16[16,128,128]{2,1,0:T(8,128)(2,1)}), bf16[16,128,128]{2,1,0:T(8,128)(2,1)S(1)}, u32[]{:S(2)}, u32[]{:S(2)}) async-start(bf16[16,128,128]{2,1,0:T(8,128)(2,1)} %fusion.6), calls=%async_computation.3 | async-start | bytes 1048576 | tf_op jit(solution)/shard_map/all_to_all | solution.py:17
  218.8 0.8 copy.49
  219.6 0.8 copy.50
  220.4 0.8 copy.51
  222.0 25.3 %all-to-all-done.3 = bf16[16,128,128]{2,1,0:T(8,128)(2,1)S(1)} async-done(((bf16[16,128,128]{2,1,0:T(8,128)(2,1)}), bf16[16,128,128]{2,1,0:T(8,128)(2,1)S(1)}, u32[]{:S(2)}, u32[]{:S(2)}) %all-to-all-start.3) | async-done | bytes 524320 | tf_op jit(solution)/shard_map/all_to_all | solution.py:17
  (94 shorter events, 12.1 us)
Async XLA Ops:
  0.6 62.2 %copy-start.5 = (f32[64,32,128]{2,1,0:T(8,128)S(1)}, f32[64,32,128]{2,1,0:T(8,128)}, u32[]{:S(2)}) copy-start(f32[64,32,128]{2,1,0:T(8,128)} %param.16) | copy-start | bytes 3145732
  0.6 62.3 %copy-start.14 = (f32[32,128]{1,0:T(8,128)S(1)}, f32[32,128]{1,0:T(8,128)}, u32[]{:S(2)}) copy-start(f32[32,128]{1,0:T(8,128)} %param.19) | copy-start | bytes 49156
  0.7 62.3 %copy-start.22 = (f32[128]{0:T(128)S(1)}, f32[128]{0:T(128)}, u32[]{:S(2)}) copy-start(f32[128]{0:T(128)} %param.11) | copy-start | bytes 1540
  0.7 62.3 %copy-start.18 = (f32[32,128]{1,0:T(8,128)S(1)}, f32[32,128]{1,0:T(8,128)}, u32[]{:S(2)}) copy-start(f32[32,128]{1,0:T(8,128)} %param.17) | copy-start | bytes 49156
  0.7 62.3 %copy-start.19 = (f32[32,128]{1,0:T(8,128)S(1)}, f32[32,128]{1,0:T(8,128)}, u32[]{:S(2)}) copy-start(f32[32,128]{1,0:T(8,128)} %param.18) | copy-start | bytes 49156
  2.3 15.1 %all-to-all-start = ((f32[16,1,256]{2,1,0:T(1,128)}), f32[16,1,256]{2,1,0:T(1,128)S(1)}, u32[]{:S(2)}, u32[]{:S(2)}) async-start(f32[16,1,256]{2,1,0:T(1,128)} %broadcast_in_dim.51), calls=%async_computation | async-start | bytes 32768 | tf_op jit(solution)/shard_map/all_to_all | solution.py:17
  19.1 74.6 %all-to-all-start.1 = ((bf16[16,144,128]{2,1,0:T(8,128)(2,1)}), bf16[16,144,128]{2,1,0:T(8,128)(2,1)}, u32[]{:S(2)}, u32[]{:S(2)}) async-start(bf16[16,144,128]{2,1,0:T(8,128)(2,1)} %broadcast_in_dim.52), calls=%async_computation.1 | async-start | bytes 1179648 | tf_op jit(solution)/shard_map/all_to_all | solution.py:17
  62.8 1.2 copy-start.6
  63.0 0.6 copy-start.11
  63.0 39.4 %copy-start.9 = (bf16[32,128]{1,0:T(8,128)(2,1)}, bf16[32,128]{1,0:T(8,128)(2,1)S(1)}, u32[]{:S(2)}) copy-start(bf16[32,128]{1,0:T(8,128)(2,1)S(1)} %get-tuple-element.39) | copy-start | bytes 24580
  93.7 112.6 %all-to-all-start.2 = ((bf16[16,5,96,128]{3,2,1,0:T(8,128)(2,1)}), bf16[16,5,96,128]{3,2,1,0:T(8,128)(2,1)S(1)}, u32[]{:S(2)}, u32[]{:S(2)}) async-start(bf16[16,5,96,128]{3,2,1,0:T(8,128)(2,1)} %pad_maximum_fusion), calls=%async_computation.2 | async-start | bytes 3932160 | tf_op jit(solution)/shard_map/all_to_all | solution.py:17
  101.4 1.0 copy-start.12
  101.5 3.8 %copy-start.15 = (f32[32,128]{1,0:T(8,128)S(1)}, f32[32,128]{1,0:T(8,128)}, u32[]{:S(2)}) copy-start(f32[32,128]{1,0:T(8,128)} %param.19) | copy-start | bytes 49156
  103.3 6.7 %collective-permute-start = (bf16[2112,128]{1,0:T(8,128)(2,1)}, bf16[2112,128]{1,0:T(8,128)(2,1)}, u32[]{:S(2)}, u32[]{:S(2)}) collective-permute-start(bf16[2112,128]{1,0:T(8,128)(2,1)} %bitcast.5), channel_id=1, source_target_pairs={{0,1},{1,0},{2,3},{3,2},{4,5},{5,4},{6,7},{7,6},{8,9},{9,8},{10,11... | collective-permute-start | bytes 1622024 | tf_op jit(solution)/shard_map/ppermute | solution.py:42
  105.2 6.5 %copy-start.1 = (bf16[32,64,128]{2,1,0:T(8,128)(2,1)S(1)}, bf16[32,64,128]{2,1,0:T(8,128)(2,1)}, u32[]{:S(2)}) copy-start(bf16[32,64,128]{2,1,0:T(8,128)(2,1)} %get-tuple-element.29) | copy-start | bytes 1572868
  105.3 3.7 %collective-permute-start.1 = (bf16[1056,128]{1,0:T(8,128)(2,1)S(1)}, bf16[1056,128]{1,0:T(8,128)(2,1)S(1)}, u32[]{:S(2)}, u32[]{:S(2)}) collective-permute-start(bf16[1056,128]{1,0:T(8,128)(2,1)S(1)} %bitcast.107), channel_id=1, source_target_pairs={{0,1},{1,0},{2,3},{3,2},{4,5},{5,4},{6,7},{7,6},{8,9},{9,8},{10,11... | collective-permute-start | bytes 811016 | tf_op jit(solution)/shard_map/ppermute | solution.py:42
  108.1 9.5 %copy-start.16 = (s32[768]{0:T(1024)}, s32[768]{0:T(1024)S(1)}, u32[]{:S(2)}) copy-start(s32[768]{0:T(1024)S(1)} %eq.60) | copy-start | bytes 9220
  108.1 8.6 %copy-start.20 = (s32[32]{0:T(128)}, s32[32]{0:T(128)S(1)}, u32[]{:S(2)}) copy-start(s32[32]{0:T(128)S(1)} %iota_add_fusion) | copy-start | bytes 388
  109.1 2.9 %copy-start.8 = (bf16[1056,128]{1,0:T(8,128)(2,1)}, bf16[1056,128]{1,0:T(8,128)(2,1)S(1)}, u32[]{:S(2)}) copy-start(bf16[1056,128]{1,0:T(8,128)(2,1)S(1)} %collective-permute-done.1) | copy-start | bytes 811012
  113.0 5.6 %collective-permute-start.2 = (bf16[16,128,128]{2,1,0:T(8,128)(2,1)S(1)}, bf16[16,128,128]{2,1,0:T(8,128)(2,1)S(1)}, u32[]{:S(2)}, u32[]{:S(2)}) collective-permute-start(bf16[16,128,128]{2,1,0:T(8,128)(2,1)S(1)} %slice.105), channel_id=1, source_target_pairs={{0,1},{1,0},{2,3},{3,2},{4,5},{5,4},{6,7},{7,6},{8,9},{9,8},{10,11... | collective-permute-start | bytes 1572872 | tf_op jit(solution)/shard_map/ppermute | solution.py:42
  116.8 0.6 copy-start.7
  117.6 1.1 copy-start
  120.4 0.8 copy-start.10
  120.5 0.8 copy-start.13
  121.6 2.3 copy-start.3
  123.9 36.6 %copy-start.21 = (s32[32]{0:T(128)S(1)}, s32[32]{0:T(128)}, u32[]{:S(2)}) copy-start(s32[32]{0:T(128)} %copy-done.20) | copy-start | bytes 388
  123.9 37.8 %copy-start.17 = (s32[768]{0:T(1024)S(1)}, s32[768]{0:T(1024)}, u32[]{:S(2)}) copy-start(s32[768]{0:T(1024)} %copy-done.16) | copy-start | bytes 9220
  125.0 21.7 %collective-permute-start.3 = (bf16[832,128]{1,0:T(8,128)(2,1)}, bf16[832,128]{1,0:T(8,128)(2,1)}, u32[]{:S(2)}, u32[]{:S(2)}) collective-permute-start(bf16[832,128]{1,0:T(8,128)(2,1)} %get-tuple-element.23), channel_id=1, source_target_pairs={{0,8},{2,10},{4,12},{6,14},{8,0},{10,2},{12,4},{14,6},{1,9},{3,11}... | collective-permute-start | bytes 638984 | tf_op jit(solution)/shard_map/ppermute | solution.py:22
  127.6 29.5 %collective-permute-start.4 = (bf16[832,128]{1,0:T(8,128)(2,1)}, bf16[832,128]{1,0:T(8,128)(2,1)}, u32[]{:S(2)}, u32[]{:S(2)}) collective-permute-start(bf16[832,128]{1,0:T(8,128)(2,1)} %get-tuple-element.24), channel_id=1, source_target_pairs={{0,6},{2,8},{4,10},{6,12},{8,14},{10,0},{12,2},{14,4},{1,7},{3,9},... | collective-permute-start | bytes 638984 | tf_op jit(solution)/shard_map/ppermute | solution.py:22
  132.7 30.9 %collective-permute-start.5 = (bf16[832,128]{1,0:T(8,128)(2,1)}, bf16[832,128]{1,0:T(8,128)(2,1)}, u32[]{:S(2)}, u32[]{:S(2)}) collective-permute-start(bf16[832,128]{1,0:T(8,128)(2,1)} %get-tuple-element.25), channel_id=1, source_target_pairs={{0,10},{2,12},{4,14},{6,0},{8,2},{10,4},{12,6},{14,8},{1,11},{3,13... | collective-permute-start | bytes 638984 | tf_op jit(solution)/shard_map/ppermute | solution.py:22
  136.5 27.1 %collective-permute-start.6 = (bf16[832,128]{1,0:T(8,128)(2,1)}, bf16[832,128]{1,0:T(8,128)(2,1)}, u32[]{:S(2)}, u32[]{:S(2)}) collective-permute-start(bf16[832,128]{1,0:T(8,128)(2,1)} %get-tuple-element.26), channel_id=1, source_target_pairs={{0,4},{2,6},{4,8},{6,10},{8,12},{10,14},{12,0},{14,2},{1,5},{3,7},... | collective-permute-start | bytes 638984 | tf_op jit(solution)/shard_map/ppermute | solution.py:22
  140.8 23.6 %collective-permute-start.7 = (bf16[832,128]{1,0:T(8,128)(2,1)}, bf16[832,128]{1,0:T(8,128)(2,1)}, u32[]{:S(2)}, u32[]{:S(2)}) collective-permute-start(bf16[832,128]{1,0:T(8,128)(2,1)} %get-tuple-element.27), channel_id=1, source_target_pairs={{0,12},{2,14},{4,0},{6,2},{8,4},{10,6},{12,8},{14,10},{1,13},{3,15... | collective-permute-start | bytes 638984 | tf_op jit(solution)/shard_map/ppermute | solution.py:22
  146.7 21.9 %collective-permute-start.8 = (bf16[832,128]{1,0:T(8,128)(2,1)}, bf16[832,128]{1,0:T(8,128)(2,1)}, u32[]{:S(2)}, u32[]{:S(2)}) collective-permute-start(bf16[832,128]{1,0:T(8,128)(2,1)} %get-tuple-element.28), channel_id=1, source_target_pairs={{0,2},{2,4},{4,6},{6,8},{8,10},{10,12},{12,14},{14,0},{1,3},{3,5},... | collective-permute-start | bytes 638984 | tf_op jit(solution)/shard_map/ppermute | solution.py:22
  157.1 11.5 %collective-permute-start.9 = (bf16[832,128]{1,0:T(8,128)(2,1)}, bf16[832,128]{1,0:T(8,128)(2,1)}, u32[]{:S(2)}, u32[]{:S(2)}) collective-permute-start(bf16[832,128]{1,0:T(8,128)(2,1)} %fusion.33), channel_id=1, source_target_pairs={{0,14},{2,0},{4,2},{6,4},{8,6},{10,8},{12,10},{14,12},{1,15},{3,1}... | collective-permute-start | bytes 638984 | tf_op jit(solution)/shard_map/ppermute | solution.py:22
  160.5 8.1 %copy-start.4 = (bf16[8,64,128]{2,1,0:T(8,128)(2,1)S(1)}, bf16[8,64,128]{2,1,0:T(8,128)(2,1)}, u32[]{:S(2)}) copy-start(bf16[8,64,128]{2,1,0:T(8,128)(2,1)} %copy-done.3) | copy-start | bytes 393220
  170.3 26.8 %copy-start.2 = (bf16[32,32,256]{2,1,0:T(8,128)(2,1)S(1)}, bf16[32,32,256]{2,1,0:T(8,128)(2,1)}, u32[]{:S(2)}) copy-start(bf16[32,32,256]{2,1,0:T(8,128)(2,1)} %pad_maximum_fusion.5) | copy-start | bytes 1572868
  199.0 0.7 slice-start
  199.0 1.0 copy-start.23
  201.5 3.8 %collective-permute-start.10 = (bf16[2048,128]{1,0:T(8,128)(2,1)S(1)}, bf16[2048,128]{1,0:T(8,128)(2,1)S(1)}, u32[]{:S(2)}, u32[]{:S(2)}) collective-permute-start(bf16[2048,128]{1,0:T(8,128)(2,1)S(1)} %bitcast.104), channel_id=1, source_target_pairs={{0,1},{1,0},{2,3},{3,2},{4,5},{5,4},{6,7},{7,6},{8,9},{9,8},{10,11... | collective-permute-start | bytes 1572872 | tf_op jit(solution)/shard_map/ppermute | solution.py:42
  206.3 41.0 %all-to-all-start.3 = ((bf16[16,128,128]{2,1,0:T(8,128)(2,1)}), bf16[16,128,128]{2,1,0:T(8,128)(2,1)S(1)}, u32[]{:S(2)}, u32[]{:S(2)}) async-start(bf16[16,128,128]{2,1,0:T(8,128)(2,1)} %fusion.6), calls=%async_computation.3 | async-start | bytes 1048576 | tf_op jit(solution)/shard_map/all_to_all | solution.py:17
